TPU v7x, 32 devices: a whole 2x2x4 slice. The times are simulated.
32 devices in a mesh: grp: 2 (over y), sp: 4 (over z), tp: 4 (over x, core).
Axes of the slice: x: 2, y: 2, z: 4, core: 2. Of those that a mesh axis runs over, the one named last changes fastest.
Arguments:
- tokens: bfloat16 [1024, 2048], P(('grp', 'sp'), 'tp'), parts along dimension 0, may hold values from -30 to 30, as said below
- norm_gain: float32 [2, 2048], replicated, may hold values from 0.1 to 1.9
- in_weight: bfloat16 [2, 2048, 2048], P(None, 'sp', 'tp'), may hold values from -0.125 to 0.125
- gate_weight: bfloat16 [2, 2048, 2048], P(None, 'sp', 'tp'), may hold values from -0.125 to 0.125
- conv_taps: float32 [2, 4, 2048], P(None, None, 'tp'), may hold values from -3 to 3
- decay_logit: float32 [2, 2, 2048], P(None, None, 'tp'), may hold values from 4 to 20, as said below
- gate_maps: bfloat16 [2, 2048, 1024], P(None, 'tp', 'sp'), may hold values from -0.375 to 0.375
- out_weight: bfloat16 [2, 2048, 2048], P(None, 'sp', 'tp'), may hold values from -0.375 to 0.375
- final_gain: float32 [2048], P('tp'), may hold values from 0.1 to 1.9
Outputs:
- normed_out: bfloat16 [1024, 2048], P(('grp', 'sp'), 'tp'), parts along dimension 0
There are 2 independent parts, one for each index of `grp`. A program takes and returns all parts, laid end to end along the dimension named above; an argument that names none is the same for every part. Nothing has to cross between parts.
Inputs may be any that keep to these rules, and one draw needn't show every extreme that they name: Activations of order one whose scale changes by blocks of tokens and of channels. `decay_logit`: decay parameters; channels differ in how far their state reaches.
All inputs are finite; a program needn't handle non-finite values.
Results may differ from a plain program's by a relative error of at most 0.02.
Values may be sent and summed in bfloat16 or wider, within the bound.
No kernel may reach another device: no remote copies, remote signals or barrier semaphores. Data moves between devices by JAX's collectives and lax.ppermute only.
A program may use at most 128 MiB of HBM per device.

v0:
```python
import jax
import jax.numpy as jnp
from jax import lax
from jax.sharding import PartitionSpec as P

D = 2048
HEAD_W = 256
TAPS = 4
LAYERS = 2


EPS = 1e-06


def extended(value, sides, width):
    for axis, dim in sides:
        devices, length = (lax.axis_size(axis), value.shape[dim])
        up = [(i, (i + 1) % devices) for i in range(devices - 1)]
        down = [(j, i) for i, j in up]
        last = lax.slice_in_dim(value, length - width, length, axis=dim)
        leading = lax.slice_in_dim(value, 0, width, axis=dim)
        before = lax.ppermute(last, axis, up)
        after = lax.ppermute(leading, axis, down)
        value = jnp.concatenate([before, value, after], axis=dim)
    return value


def combine_pair(earlier, later):
    return (earlier[0] * later[0], later[0] * earlier[1] + later[1])


def body(
    tokens,
    norm_gain,
    in_weight,
    gate_weight,
    conv_taps,
    decay_logit,
    gate_maps,
    out_weight,
    final_gain,
):
    resid = tokens
    rows = tokens.shape[0]
    width = in_weight.shape[2]
    local_heads = width // HEAD_W
    for layer in range(LAYERS):
        whole = lax.all_gather(resid, "tp", axis=1, tiled=True)
        wide = whole.astype(jnp.float32)
        normed = (
            wide * lax.rsqrt(jnp.mean(wide * wide, axis=1, keepdims=True) + EPS) * norm_gain[layer]
        ).astype(jnp.bfloat16)
        proj_in = jnp.dot(
            normed,
            lax.all_gather(in_weight[layer], "sp", axis=0, tiled=True),
            preferred_element_type=jnp.float32,
        )
        proj_gate = jnp.dot(
            normed,
            lax.all_gather(gate_weight[layer], "sp", axis=0, tiled=True),
            preferred_element_type=jnp.float32,
        )
        xin = proj_in.astype(jnp.bfloat16)
        gin = proj_gate.astype(jnp.bfloat16)
        padded = extended(xin, (("sp", 0),), 2).astype(jnp.float32)
        conv = conv_taps[layer, 0] * padded[0:rows]
        for k in range(1, TAPS):
            conv = conv + conv_taps[layer, k] * padded[k : k + rows]
        conv = conv.astype(jnp.bfloat16)
        stacked = conv.reshape(rows, local_heads, HEAD_W)
        piece = lax.all_gather(gate_maps[layer], "sp", axis=1, tiled=True)
        blocks = piece.reshape(local_heads, HEAD_W, piece.shape[1])
        pre = jnp.einsum("thi,hij->thj", stacked, blocks, preferred_element_type=jnp.float32)
        pre = pre.reshape(rows, local_heads, 4, HEAD_W)
        conv32 = conv.astype(jnp.float32)
        locals_a = []
        locals_h = []
        for direction in range(2):
            rate = jax.nn.sigmoid(pre[:, :, 2 * direction]).reshape(rows, width)
            inp = jax.nn.sigmoid(pre[:, :, 2 * direction + 1]).reshape(rows, width)
            log_a = -8.0 * rate * jax.nn.softplus(-decay_logit[layer, direction])
            decay = jnp.exp(log_a)
            drive = jnp.sqrt(-jnp.expm1(2.0 * log_a)) * inp * conv32
            prod_a, state = lax.associative_scan(
                combine_pair, (decay, drive), reverse=direction == 1, axis=0
            )
            locals_a.append(prod_a)
            locals_h.append(state)
        summary = jnp.stack([locals_a[0][-1], locals_h[0][-1], locals_a[1][0], locals_h[1][0]])[
            None
        ]
        every = lax.all_gather(summary, "sp", axis=0, tiled=True)
        count = every.shape[0]
        me = lax.axis_index("sp")
        _, incl_f = lax.associative_scan(combine_pair, (every[:, 0], every[:, 1]), axis=0)
        _, incl_b = lax.associative_scan(
            combine_pair, (every[:, 2], every[:, 3]), reverse=True, axis=0
        )
        before = lax.dynamic_index_in_dim(incl_f, jnp.maximum(me - 1, 0), 0, keepdims=False)
        after = lax.dynamic_index_in_dim(incl_b, jnp.minimum(me + 1, count - 1), 0, keepdims=False)
        carry_f = before * (me > 0).astype(jnp.float32)
        carry_b = after * (me < count - 1).astype(jnp.float32)
        hidden = locals_h[0] + locals_a[0] * carry_f + locals_h[1] + locals_a[1] * carry_b
        mix = (jax.nn.gelu(gin.astype(jnp.float32)) * hidden).astype(jnp.bfloat16)
        full_mix = lax.all_gather(mix, "tp", axis=1, tiled=True)
        out = jnp.dot(
            full_mix,
            lax.all_gather(out_weight[layer], "sp", axis=0, tiled=True),
            preferred_element_type=jnp.float32,
        )
        resid = (resid.astype(jnp.float32) + out).astype(jnp.bfloat16)
    wide = resid.astype(jnp.float32)
    total = lax.psum(jnp.sum(wide * wide, axis=1), "tp")
    scale = lax.rsqrt(total / D + EPS)
    return (wide * scale[:, None] * final_gain).astype(jnp.bfloat16)


def solution(mesh):
    placed = (
        P(("grp", "sp"), "tp"),
        P(),
        P(None, "sp", "tp"),
        P(None, "sp", "tp"),
        P(None, None, "tp"),
        P(None, None, "tp"),
        P(None, "tp", "sp"),
        P(None, "sp", "tp"),
        P("tp"),
    )
    return jax.shard_map(
        body, mesh=mesh, in_specs=placed, out_specs=P(("grp", "sp"), "tp"), check_vma=False
    )
```

profile of v0, /device:TPU:0, one launch (start us, length us, event | category | flops | bytes accessed | tf_op | source)
XLA Modules:
  0.0 364.2 jit_solution(13427582428393918991)
XLA Ops:
  6.5 2.4 fusion.182
  9.0 0.8 fusion.184
  9.9 1.1 fusion.183
  11.1 1.1 fusion.179
  12.2 0.5 all-gather.31.cloned.1.call-update
  12.8 0.5 all-gather.33.cloned.1.call-update
  13.4 0.7 all-gather.29.cloned.1.call-update
  14.1 0.7 all-gather.35.cloned.1.call-update
  14.9 8.6 %all_gather.42 = bf16[128,2048]{1,0:T(8,128)(2,1)S(1)} all-gather(bf16[128,512]{1,0:T(8,128)(2,1)S(1)} %copy-done.2), channel_id=1, replica_groups=mesh['grp'=2,'sp'=4,'tp'=4] {'tp'}, dimensions={1}, use_global_device_ids=true | all-gather | bytes 655360 | tf_op jit(solution)/shard_map/all_gather | solution.py:48
  23.5 0.2 fusion.45
  23.8 33.7 %all-gather.23.cloned.1.call-done = bf16[1,2048,512]{2,1,0:T(8,128)(2,1)} async-done(((bf16[1,512,512]{2,1,0:T(8,128)(2,1)}), bf16[1,2048,512]{2,1,0:T(8,128)(2,1)}) %all-gather.23.cloned.1.call-update) | async-done | bytes 2097168 | tf_op jit(solution)/shard_map/all_gather | solution.py:55
  57.5 2.1 fusion.33
  59.6 2.1 collective-permute-start
  61.7 1.3 collective-permute-start.1
  63.0 4.1 %collective-permute-done.1 = bf16[2,512]{1,0:T(2,128)(2,1)S(1)} collective-permute-done((bf16[2,512]{1,0:T(2,128)(2,1)S(1)}, bf16[2,512]{1,0:T(2,128)(2,1)S(1)}, u32[]{:S(2)}, u32[]{:S(2)}) %collective-permute-start.1) | collective-permute-done | bytes 2080 | tf_op jit(solution)/shard_map/ppermute | solution.py:23
  67.3 20.5 %all-gather.25.cloned.1.call-done = bf16[1,512,1024]{2,1,0:T(8,128)(2,1)} async-done(((bf16[1,512,256]{2,1,0:T(8,128)(2,1)}), bf16[1,512,1024]{2,1,0:T(8,128)(2,1)}) %all-gather.25.cloned.1.call-update) | async-done | bytes 1048592 | tf_op jit(solution)/shard_map/all_gather | solution.py:71
  87.8 1.5 convolution_bitcast_fusion.1
  89.4 0.5 reshape.178
  89.9 0.8 fusion.181
  90.6 0.6 fusion.103
  91.3 0.6 fusion.109
  91.9 0.5 convert_multiply_fusion.7
  93.8 0.2 slice.1270
  94.0 0.2 slice.1319
  98.3 0.2 slice.1371
  98.5 0.2 slice.1408
  99.0 13.7 %all-gather.10 = f32[4,4,512]{2,1,0:T(4,128)S(1)} all-gather(f32[1,4,512]{2,1,0:T(4,128)S(1)} %maximum_bitcast_fusion), channel_id=5, replica_groups=mesh['grp'=2,'sp'=4,'tp'=4] {'sp'}, dimensions={0}, use_global_device_ids=true | all-gather | bytes 40960 | tf_op jit(solution)/shard_map/all_gather | solution.py:92
  114.1 0.1 rev.12
  114.2 0.1 rev.13
  114.4 19.5 %all-gather.21.cloned.1.call-done = bf16[1,2048,512]{2,1,0:T(8,128)(2,1)} async-done(((bf16[1,512,512]{2,1,0:T(8,128)(2,1)}), bf16[1,2048,512]{2,1,0:T(8,128)(2,1)}) %all-gather.21.cloned.1.call-update) | async-done | bytes 2097168 | tf_op jit(solution)/shard_map/all_gather | solution.py:60
  133.9 2.2 fusion.63
  136.1 7.2 %all_gather.47 = bf16[128,2048]{1,0:T(8,128)(2,1)S(1)} all-gather(bf16[128,512]{1,0:T(8,128)(2,1)S(1)} %fusion.63), channel_id=1, replica_groups=mesh['grp'=2,'sp'=4,'tp'=4] {'tp'}, dimensions={1}, use_global_device_ids=true | all-gather | bytes 655360 | tf_op jit(solution)/shard_map/all_gather | solution.py:105
  143.2 36.6 %all-gather.27.cloned.1.call-done = bf16[1,2048,512]{2,1,0:T(8,128)(2,1)} async-done(((bf16[1,512,512]{2,1,0:T(8,128)(2,1)}), bf16[1,2048,512]{2,1,0:T(8,128)(2,1)}) %all-gather.27.cloned.1.call-update) | async-done | bytes 2097168 | tf_op jit(solution)/shard_map/all_gather | solution.py:108
  179.8 2.0 fusion.24
  181.9 7.3 %all_gather.49 = bf16[128,2048]{1,0:T(8,128)(2,1)S(1)} all-gather(bf16[128,512]{1,0:T(8,128)(2,1)S(1)} %fusion.24), channel_id=1, replica_groups=mesh['grp'=2,'sp'=4,'tp'=4] {'tp'}, dimensions={1}, use_global_device_ids=true | all-gather | bytes 655360 | tf_op jit(solution)/shard_map/all_gather | solution.py:48
  189.2 0.2 fusion.48
  189.4 36.3 %all-gather.31.cloned.1.call-done = bf16[1,2048,512]{2,1,0:T(8,128)(2,1)} async-done(((bf16[1,512,512]{2,1,0:T(8,128)(2,1)}), bf16[1,2048,512]{2,1,0:T(8,128)(2,1)}) %all-gather.31.cloned.1.call-update) | async-done | bytes 2097168 | tf_op jit(solution)/shard_map/all_gather | solution.py:55
  225.7 2.1 fusion.42
  227.8 2.1 collective-permute-start.2
  229.9 1.3 collective-permute-start.3
  231.3 4.1 %collective-permute-done.3 = bf16[2,512]{1,0:T(2,128)(2,1)S(1)} collective-permute-done((bf16[2,512]{1,0:T(2,128)(2,1)S(1)}, bf16[2,512]{1,0:T(2,128)(2,1)S(1)}, u32[]{:S(2)}, u32[]{:S(2)}) %collective-permute-start.3) | collective-permute-done | bytes 2080 | tf_op jit(solution)/shard_map/ppermute | solution.py:23
  235.6 20.3 %all-gather.33.cloned.1.call-done = bf16[1,512,1024]{2,1,0:T(8,128)(2,1)} async-done(((bf16[1,512,256]{2,1,0:T(8,128)(2,1)}), bf16[1,512,1024]{2,1,0:T(8,128)(2,1)}) %all-gather.33.cloned.1.call-update) | async-done | bytes 1048592 | tf_op jit(solution)/shard_map/all_gather | solution.py:71
  255.9 1.5 convolution_bitcast_fusion
  257.5 0.5 reshape.181
  258.0 0.8 fusion.180
  258.7 0.3 fusion.100
  259.1 0.3 fusion.97
  259.4 0.3 fusion.94
  259.7 0.3 fusion.91
  260.0 0.5 convert_multiply_fusion.5
  261.9 0.2 slice.1465
  262.1 0.2 slice.1514
  266.5 0.2 slice.1566
  266.6 0.2 slice.1603
  267.2 13.7 %all-gather.11 = f32[4,4,512]{2,1,0:T(4,128)S(1)} all-gather(f32[1,4,512]{2,1,0:T(4,128)S(1)} %maximum_bitcast_fusion.1), channel_id=10, replica_groups=mesh['grp'=2,'sp'=4,'tp'=4] {'sp'}, dimensions={0}, use_global_device_ids=true | all-gather | bytes 40960 | tf_op jit(solution)/shard_map/all_gather | solution.py:92
  282.2 0.1 rev.29
  282.4 0.1 rev.30
  282.5 19.5 %all-gather.29.cloned.1.call-done = bf16[1,2048,512]{2,1,0:T(8,128)(2,1)} async-done(((bf16[1,512,512]{2,1,0:T(8,128)(2,1)}), bf16[1,2048,512]{2,1,0:T(8,128)(2,1)}) %all-gather.29.cloned.1.call-update) | async-done | bytes 2097168 | tf_op jit(solution)/shard_map/all_gather | solution.py:60
  302.0 2.2 fusion.78
  304.2 7.1 %all_gather.54 = bf16[128,2048]{1,0:T(8,128)(2,1)S(1)} all-gather(bf16[128,512]{1,0:T(8,128)(2,1)S(1)} %fusion.78), channel_id=1, replica_groups=mesh['grp'=2,'sp'=4,'tp'=4] {'tp'}, dimensions={1}, use_global_device_ids=true | all-gather | bytes 655360 | tf_op jit(solution)/shard_map/all_gather | solution.py:105
  311.3 36.7 %all-gather.35.cloned.1.call-done = bf16[1,2048,512]{2,1,0:T(8,128)(2,1)} async-done(((bf16[1,512,512]{2,1,0:T(8,128)(2,1)}), bf16[1,2048,512]{2,1,0:T(8,128)(2,1)}) %all-gather.35.cloned.1.call-update) | async-done | bytes 2097168 | tf_op jit(solution)/shard_map/all_gather | solution.py:108
  348.1 2.1 multiply_reduce_fusion
  350.2 6.4 %psum.7 = f32[128]{0:T(128)S(1)} all-reduce(f32[128]{0:T(128)S(1)} %get-tuple-element.195), channel_id=1, replica_groups=mesh['grp'=2,'sp'=4,'tp'=4] {'tp'}, use_global_device_ids=true, to_apply=%region_3.4 | all-reduce | flops 128 | bytes 1024 | tf_op jit(solution)/shard_map/psum | solution.py:113
  356.6 0.8 multiply_convert_fusion
  (560 shorter events, 12.8 us)
Async XLA Ops:
  6.5 2.5 copy-start.3
  6.5 3.4 copy-start
  6.5 51.0 %all-gather.23.cloned.1.call-start = ((), (), s32[]{:S(2)}) async-start(), calls=%async_computation.1 | async-start | bytes 2621440 | tf_op jit(solution)/shard_map/all_gather | solution.py:55
  9.0 2.1 copy-start.1
  9.0 78.8 %all-gather.25.cloned.1.call-start = ((), (), s32[]{:S(2)}) async-start(), calls=%async_computation.2 | async-start | bytes 1310720 | tf_op jit(solution)/shard_map/all_gather | solution.py:71
  9.9 124.0 %all-gather.21.cloned.1.call-start = ((), (), s32[]{:S(2)}) async-start(), calls=%async_computation | async-start | bytes 2621440 | tf_op jit(solution)/shard_map/all_gather | solution.py:60
  11.0 3.8 %copy-start.2 = (bf16[128,512]{1,0:T(8,128)(2,1)S(1)}, bf16[128,512]{1,0:T(8,128)(2,1)}, u32[]{:S(2)}) copy-start(bf16[128,512]{1,0:T(8,128)(2,1)} %param.9) | copy-start | bytes 393220
  11.0 168.8 %all-gather.27.cloned.1.call-start = ((), (), s32[]{:S(2)}) async-start(), calls=%async_computation.3 | async-start | bytes 2621440 | tf_op jit(solution)/shard_map/all_gather | solution.py:108
  12.1 11.6 %copy-start.4 = (f32[2,2048]{1,0:T(2,128)S(1)}, f32[2,2048]{1,0:T(2,128)}, u32[]{:S(2)}) copy-start(f32[2,2048]{1,0:T(2,128)} %param.10) | copy-start | bytes 49156
  12.2 11.6 %copy-start.5 = (f32[2,4,512]{2,1,0:T(4,128)S(1)}, f32[2,4,512]{2,1,0:T(4,128)}, u32[]{:S(2)}) copy-start(f32[2,4,512]{2,1,0:T(4,128)} %param.13) | copy-start | bytes 49156
  12.2 11.6 %copy-start.6 = (f32[2,2,512]{2,1,0:T(2,128)S(1)}, f32[2,2,512]{2,1,0:T(2,128)}, u32[]{:S(2)}) copy-start(f32[2,2,512]{2,1,0:T(2,128)} %param.14) | copy-start | bytes 24580
  12.2 213.6 %all-gather.31.cloned.1.call-start = ((), (), s32[]{:S(2)}) async-start(), calls=%async_computation.5 | async-start | bytes 2621440 | tf_op jit(solution)/shard_map/all_gather | solution.py:55
  12.8 243.2 %all-gather.33.cloned.1.call-start = ((), (), s32[]{:S(2)}) async-start(), calls=%async_computation.6 | async-start | bytes 1310720 | tf_op jit(solution)/shard_map/all_gather | solution.py:71
  13.3 288.7 %all-gather.29.cloned.1.call-start = ((), (), s32[]{:S(2)}) async-start(), calls=%async_computation.4 | async-start | bytes 2621440 | tf_op jit(solution)/shard_map/all_gather | solution.py:60
  14.1 334.0 %all-gather.35.cloned.1.call-start = ((), (), s32[]{:S(2)}) async-start(), calls=%async_computation.7 | async-start | bytes 2621440 | tf_op jit(solution)/shard_map/all_gather | solution.py:108
  59.6 3.4 collective-permute-start
  61.7 5.5 %collective-permute-start.1 = (bf16[2,512]{1,0:T(2,128)(2,1)S(1)}, bf16[2,512]{1,0:T(2,128)(2,1)S(1)}, u32[]{:S(2)}, u32[]{:S(2)}) collective-permute-start(bf16[2,512]{1,0:T(2,128)(2,1)S(1)} %get-tuple-element.52), channel_id=1, source_target_pairs={{4,0},{8,4},{12,8},{5,1},{9,5},{13,9},{6,2},{10,6},{14,10},{7,3},{... | collective-permute-start | bytes 6152 | tf_op jit(solution)/shard_map/ppermute | solution.py:23
  227.8 3.4 collective-permute-start.2
  229.9 5.5 %collective-permute-start.3 = (bf16[2,512]{1,0:T(2,128)(2,1)S(1)}, bf16[2,512]{1,0:T(2,128)(2,1)S(1)}, u32[]{:S(2)}, u32[]{:S(2)}) collective-permute-start(bf16[2,512]{1,0:T(2,128)(2,1)S(1)} %get-tuple-element.40), channel_id=1, source_target_pairs={{4,0},{8,4},{12,8},{5,1},{9,5},{13,9},{6,2},{10,6},{14,10},{7,3},{... | collective-permute-start | bytes 6152 | tf_op jit(solution)/shard_map/ppermute | solution.py:23
  304.2 52.4 %copy-start.7 = (f32[512]{0:T(512)S(1)}, f32[512]{0:T(512)}, u32[]{:S(2)}) copy-start(f32[512]{0:T(512)} %param.17) | copy-start | bytes 6148
Sparse Core Ops, SparseCore 0:
  9.1 48.3 all-gather.22
  59.1 28.7 all-gather.24
  89.4 44.4 all-gather.20
  135.3 44.4 all-gather.26
  181.2 44.4 all-gather.30
  227.2 28.7 all-gather.32
  257.5 44.4 all-gather.28
  303.6 44.4 all-gather.34
where the time goes:
time: 365 us; the launch traced here: 364 us
  waiting for transfers between devices  234 us (64%)
  blocking collectives  64.2 us (18%)
  local copies, waits for them, and re-layouts  19.3 us (5%)
  between operations  16.7 us (5%)
  matrix products  15.7 us (4%)
  other arithmetic  7.33 us (2%)
  starting transfers between devices  7.02 us (2%)
    all_gather x2, waiting for transfers between devices, body(): lax.all_gather(out_weight[layer], 'sp', axis=0, tiled=True)  73.3 us
    all_gather x2, waiting for transfers between devices, body(): lax.all_gather(in_weight[layer], 'sp', axis=0, tiled=True)  70 us
    all_gather x2, waiting for transfers between devices, body(): piece = lax.all_gather(gate_maps[layer], 'sp', axis=1, tiled=True)  40.8 us
    all_gather x2, waiting for transfers between devices, body(): lax.all_gather(gate_weight[layer], 'sp', axis=0, tiled=True)  39 us
    all_gather x2, blocking collectives, body(): every = lax.all_gather(summary, 'sp', axis=0, tiled=True)  27.5 us
    all_gather x2, blocking collectives, body(): whole = lax.all_gather(resid, 'tp', axis=1, tiled=True)  16 us
    all_gather x2, blocking collectives, body(): full_mix = lax.all_gather(mix, 'tp', axis=1, tiled=True)  14.3 us
    ppermute x2, waiting for transfers between devices, extended(): after = lax.ppermute(leading, axis, down)  8.27 us
  transfers between devices with their start and end apart: 12, of which 10 were waited for; matrix products, arithmetic and copies ran while one was open for 10% of the time, Pallas kernels for 0%

commit v1 on v0

--- a/solution.py
+++ b/solution.py
@@ -1,15 +1,216 @@
 import jax
 import jax.numpy as jnp
 from jax import lax
+from jax.experimental import pallas as pl
+from jax.experimental.pallas import tpu as pltpu
 from jax.sharding import PartitionSpec as P
 
 D = 2048
 HEAD_W = 256
 TAPS = 4
 LAYERS = 2
-
+SEGS = 8
 
 EPS = 1e-06
+BF = jnp.bfloat16
+F32 = jnp.float32
+
+
+def conv_kernel(*refs):
+    pieces = refs[:-4]
+    scale_ref, taps_ref, conv_ref, gin_ref = refs[-4:]
+    total = pieces[0][...].astype(F32)
+    for piece in pieces[1:]:
+        total = total + piece[...].astype(F32)
+    total = total * scale_ref[...]
+    length, width = conv_ref.shape
+    gin_ref[...] = total[:, width:].astype(BF)
+    xin = total[:, :width].astype(BF).astype(F32)
+    row = lax.broadcasted_iota(jnp.int32, (length, width), 0)
+    conv = None
+    for k in range(TAPS):
+        off = k - 2
+        shifted = xin if off == 0 else pltpu.roll(xin, (-off) % length, 0)
+        if off < 0:
+            shifted = jnp.where(row >= -off, shifted, 0.0)
+        elif off > 0:
+            shifted = jnp.where(row < length - off, shifted, 0.0)
+        term = taps_ref[k : k + 1, :] * shifted
+        conv = term if conv is None else conv + term
+    conv_ref[...] = conv.astype(BF)
+
+
+def neg_expm1(y):
+    series = 1.0 + y * (1.0 / 8.0)
+    for n in range(7, 1, -1):
+        series = 1.0 + y * (1.0 / n) * series
+    return jnp.where(y > -0.5, -y * series, 1.0 - jnp.exp(y))
+
+
+def scan_kernel(head_ref, conv_ref, gin_ref, maps_ref, coef_ref, mix_ref, a0, b0, a1, b1):
+    length, width = conv_ref.shape
+    steps = length // SEGS
+    conv = conv_ref[...].astype(F32)
+    pre = jnp.dot(head_ref[...], maps_ref[...], preferred_element_type=F32)
+    for d, (a_ref, b_ref) in enumerate(((a0, b0), (a1, b1))):
+        rate = jax.nn.sigmoid(pre[:, (2 * d) * width : (2 * d + 1) * width])
+        inp = jax.nn.sigmoid(pre[:, (2 * d + 1) * width : (2 * d + 2) * width])
+        log_a = rate * coef_ref[d : d + 1, :]
+        a_ref[...] = jnp.exp(log_a)
+        b_ref[...] = jnp.sqrt(neg_expm1(2.0 * log_a)) * inp * conv
+
+    def step(j, state):
+        pf, hf, pb, hb = state
+        at = pl.ds(j, SEGS, stride=steps)
+        back = pl.ds(steps - 1 - j, SEGS, stride=steps)
+        af = a0[at, :]
+        ab = a1[back, :]
+        hf = af * hf + b0[at, :]
+        hb = ab * hb + b1[back, :]
+        pf = af * pf
+        pb = ab * pb
+        a0[at, :] = pf
+        b0[at, :] = hf
+        a1[back, :] = pb
+        b1[back, :] = hb
+        return pf, hf, pb, hb
+
+    one = jnp.ones((SEGS, width), F32)
+    zero = jnp.zeros((SEGS, width), F32)
+    pf, hf, pb, hb = lax.fori_loop(0, steps, step, (one, zero, one, zero), unroll=8)
+    carry = jnp.zeros((1, width), F32)
+    fwd = []
+    for s in range(SEGS):
+        fwd.append(carry)
+        carry = pf[s : s + 1] * carry + hf[s : s + 1]
+    carry = jnp.zeros((1, width), F32)
+    bwd = [None] * SEGS
+    for s in reversed(range(SEGS)):
+        bwd[s] = carry
+        carry = pb[s : s + 1] * carry + hb[s : s + 1]
+    for s in range(SEGS):
+        rows = slice(s * steps, (s + 1) * steps)
+        hidden = b0[rows, :] + a0[rows, :] * fwd[s] + b1[rows, :] + a1[rows, :] * bwd[s]
+        gate = jax.nn.gelu(gin_ref[rows, :].astype(F32), approximate=True)
+        mix_ref[rows, :] = (gate * hidden).astype(BF)
+
+
+def conv_call(pieces, scale, taps):
+    length, width = pieces[0].shape[0], taps.shape[1]
+    out = jax.ShapeDtypeStruct((length, width), BF)
+    return pl.pallas_call(conv_kernel, out_shape=(out, out), name="conv")(*pieces, scale, taps)
+
+
+def scan_call(head, conv, gin, maps, coef):
+    return pl.pallas_call(
+        scan_kernel,
+        out_shape=jax.ShapeDtypeStruct(conv.shape, BF),
+        scratch_shapes=[pltpu.VMEM(conv.shape, F32)] * 4,
+        name="scan",
+    )(head, conv, gin, maps, coef)
+
+
+def body_square(
+    tokens,
+    norm_gain,
+    in_weight,
+    gate_weight,
+    conv_taps,
+    decay_logit,
+    gate_maps,
+    out_weight,
+    final_gain,
+):
+    n = lax.axis_size("sp")
+    s = lax.axis_index("sp")
+    q = lax.axis_index("tp")
+    rows, block = tokens.shape
+    width = block // n
+    group = HEAD_W // width
+    axes = ("sp", "tp")
+    swap = [(a * n + b, b * n + a) for a in range(n) for b in range(n)]
+    to_piece = [[(a * n + b, b * n + (a - k) % n) for a in range(n) for b in range(n)] for k in range(n)]
+    rotate = [[(a, (a + k) % n) for a in range(n)] for k in range(n)]
+    sets = [[g * group + i for i in range(group)] for g in range(n // group)]
+
+    def scatter(make):
+        return [lax.ppermute(make((s - k) % n), axes, to_piece[k]) for k in range(n)]
+
+    def cols(value, at, size):
+        return lax.dynamic_slice_in_dim(value, at * size, size, value.ndim - 1)
+
+    turned = lax.ppermute(tokens, axes, swap)
+    small = jnp.concatenate([conv_taps, decay_logit], axis=1)
+    small = cols(lax.ppermute(small, axes, swap), q, width)
+    full = lax.all_gather(turned, "tp", axis=0, tiled=True)
+    own = cols(full, q, width)
+    gain = cols(norm_gain, s, block)
+
+    def maps_of(layer):
+        held = gate_maps[layer]
+
+        def cut(piece):
+            at = (piece // group * HEAD_W, piece % group * width)
+            return lax.dynamic_slice(held, at, (HEAD_W, width))
+
+        got = scatter(cut)
+        ordered = jnp.stack(got)
+        ordered = jnp.stack([lax.dynamic_index_in_dim(ordered, (g - q) % n, 0, False) for g in range(n)], 1)
+        return ordered.reshape(HEAD_W, n * width)
+
+    for layer in range(LAYERS):
+        wide = full.astype(F32)
+        part = jnp.sum(wide * wide, axis=1)
+        total = part
+        for k in range(1, n):
+            total = total + lax.ppermute(part, "sp", rotate[k])
+        scale = lax.rsqrt(total / D + EPS)[:, None]
+        scaled = (wide * gain[layer]).astype(BF)
+
+        def project(piece):
+            w = jnp.concatenate(
+                [cols(in_weight[layer], piece, width), cols(gate_weight[layer], piece, width)], axis=1
+            )
+            return jnp.dot(scaled, w, preferred_element_type=F32).astype(BF)
+
+        conv, gin = conv_call(scatter(project), scale, small[layer, :TAPS])
+        head = conv
+        if group > 1:
+            head = lax.all_gather(conv, "tp", axis=1, tiled=True, axis_index_groups=sets)
+        coef = -8.0 * jax.nn.softplus(-small[layer, TAPS:])
+        mix = scan_call(head, conv, gin, maps_of(layer), coef)
+        mixed = lax.all_gather(mix, "tp", axis=1, tiled=True)
+        if layer + 1 < LAYERS:
+            pieces = scatter(
+                lambda piece: jnp.dot(
+                    mixed, cols(out_weight[layer], piece, width), preferred_element_type=F32
+                ).astype(BF)
+            )
+            out = own.astype(F32)
+            for piece in pieces:
+                out = out + piece.astype(F32)
+            own = out.astype(BF)
+            full = lax.all_gather(own, "tp", axis=1, tiled=True)
+        else:
+            here = (s == q).astype(F32)
+
+            def part_for(dest):
+                m = lax.dynamic_slice_in_dim(mixed, dest * rows, rows, 0)
+                r = lax.dynamic_slice_in_dim(full, dest * rows, rows, 0)
+                return jnp.dot(m, out_weight[layer], preferred_element_type=F32) + here * r.astype(F32)
+
+            sent = [lax.ppermute(part_for((s + k) % n).astype(BF), "sp", rotate[k]) for k in range(1, n)]
+            out = part_for(s)
+            for piece in sent:
+                out = out + piece.astype(F32)
+            resid = out.astype(BF)
+    wide = resid.astype(F32)
+    part = jnp.sum(wide * wide, axis=1)
+    total = part
+    for k in range(1, n):
+        total = total + lax.ppermute(part, "tp", rotate[k])
+    scale = lax.rsqrt(total / D + EPS)
+    return (wide * scale[:, None] * final_gain).astype(BF)
 
 
 def extended(value, sides, width):
@@ -127,6 +328,12 @@
         P(None, "sp", "tp"),
         P("tp"),
     )
+    n = mesh.shape["sp"]
+    square = n == mesh.shape["tp"] and n == 4 and HEAD_W % (D // (n * n)) == 0
     return jax.shard_map(
-        body, mesh=mesh, in_specs=placed, out_specs=P(("grp", "sp"), "tp"), check_vma=False
+        body_square if square else body,
+        mesh=mesh,
+        in_specs=placed,
+        out_specs=P(("grp", "sp"), "tp"),
+        check_vma=False,
     )

time: 365 us -> 251 us (0.69)
  waiting for transfers between devices: 234 us -> 108 us
  starting transfers between devices: 7.02 us -> 50.1 us
  between operations: 16.7 us -> 0.44 us
  Pallas kernels: 0 us -> 13 us
  blocking collectives: 64.2 us -> 53.9 us
  matrix products: 15.7 us -> 7.62 us
  local copies, waits for them, and re-layouts: 19.3 us -> 11.3 us
    all_gather x8 -> x0, waiting for transfers between devices: 223 us -> none  [the longest x2 73.3 us: body(): lax.all_gather(out_weight[layer], 'sp', axis=0, tiled=True)]
    ppermute x4 -> x34, waiting for transfers between devices: 8.28 us -> 108 us  [the longest x20 94 us: scatter(): lax.ppermute(make((s - k) % n), axes, to_piece[k])]
    ppermute x4 -> x34, starting transfers between devices: 6.74 us -> 50.1 us  [the longest x20 37.7 us: scatter(): lax.ppermute(make((s - k) % n), axes, to_piece[k])]
    slice x226 -> x5, local copies, waits for them, and re-layouts: 15.5 us -> 2.07 us  [the longest x1 1.06 us: maps_of(): held = gate_maps[layer]]
    pallas_call x0 -> x4, Pallas kernels: none -> 13 us  [the longest x2 8.47 us: scan_call(): pl.pallas_call(scan_kernel, out_shape=jax.ShapeDtypeStruct(conv.shape, BF...]
    dot_general x8 -> x16, matrix products: 15.7 us -> 7.62 us  [the longest x8 5.35 us: project(): return jnp.dot(scaled, w, preferred_element_type=F32).astype(BF)]
    psum x1 -> x0, blocking collectives: 6.4 us -> none  [body(): total = lax.psum(jnp.sum(wide * wide, axis=1), 'tp')]
    all_gather x6, blocking collectives: 57.8 us -> 53.9 us  [the longest x2 25.1 us: body_square(): mixed = lax.all_gather(mix, 'tp', axis=1, tiled=True)]
  transfers between devices with their start and end apart: 12 -> 34, of which waited for: 10 -> 12; matrix products, arithmetic and copies ran while one was open for 10% -> 8% of each run, Pallas kernels for 0% -> 0%
where the time goes in v1:
time: 251 us
  waiting for transfers between devices  108 us (43%)
  blocking collectives  53.9 us (21%)
  starting transfers between devices  50.1 us (20%)
  Pallas kernels  13 us (5%)
  local copies, waits for them, and re-layouts  11.3 us (5%)
  matrix products  7.62 us (3%)
  other arithmetic  6.4 us (3%)
    ppermute x20, waiting for transfers between devices, scatter(): lax.ppermute(make((s - k) % n), axes, to_piece[k])  94 us
    ppermute x20, starting transfers between devices, scatter(): lax.ppermute(make((s - k) % n), axes, to_piece[k])  37.7 us
    all_gather x2, blocking collectives, body_square(): mixed = lax.all_gather(mix, 'tp', axis=1, tiled=True)  25.1 us
    all_gather x1, blocking collectives, body_square(): full = lax.all_gather(own, 'tp', axis=1, tiled=True)  12.7 us
    ppermute x3, waiting for transfers between devices, body_square(): lax.ppermute(part_for((s + k) % n).astype(BF), 'sp', rotate[k])  11.1 us
    all_gather x1, blocking collectives, body_square(): full = lax.all_gather(turned, 'tp', axis=0, tiled=True)  8.59 us
    pallas_call x2, Pallas kernels, scan_call(): pl.pallas_call(scan_kernel, out_shape=jax.ShapeDtypeStruct(conv.shape, BF...  8.47 us
    all_gather x2, blocking collectives, body_square(): lax.all_gather(conv, 'tp', axis=1, tiled=True, axis_index_groups=sets)  7.48 us
  transfers between devices with their start and end apart: 34, of which 12 were waited for; matrix products, arithmetic and copies ran while one was open for 8% of the time, Pallas kernels for 0%

profile of v1, /device:TPU:0, one launch (start us, length us, event | category | flops | bytes accessed | tf_op | source)
XLA Modules:
  0.0 250.6 jit_solution(11041854808962106658)
XLA Ops:
  0.0 1.7 collective-permute-start
  1.7 1.3 pad_maximum_fusion.2
  3.0 2.0 collective-permute-start.8
  5.0 1.1 fusion.89
  6.2 0.7 dynamic-slice_bitcast_fusion.23
  6.9 3.6 %collective-permute-start.27 = (bf16[256,128]{1,0:T(8,128)(2,1)}, bf16[256,128]{1,0:T(8,128)(2,1)}, u32[]{:S(2)}, u32[]{:S(2)}) collective-permute-start(bf16[256,128]{1,0:T(8,128)(2,1)} %get-tuple-element.40), channel_id=1, source_target_pairs={{0,1},{1,5},{2,9},{3,13},{4,2},{5,6},{6,10},{7,14},{8,3},{9,7},{10... | collective-permute-start | bytes 196616 | tf_op jit(solution)/shard_map/ppermute | solution.py:137
  10.5 4.4 %collective-permute-start.26 = (bf16[256,128]{1,0:T(8,128)(2,1)}, bf16[256,128]{1,0:T(8,128)(2,1)}, u32[]{:S(2)}, u32[]{:S(2)}) collective-permute-start(bf16[256,128]{1,0:T(8,128)(2,1)} %get-tuple-element.41), channel_id=1, source_target_pairs={{0,2},{1,6},{2,10},{3,14},{4,3},{5,7},{6,11},{7,15},{8,0},{9,4},{1... | collective-permute-start | bytes 196616 | tf_op jit(solution)/shard_map/ppermute | solution.py:137
  15.0 2.9 %collective-permute-start.25 = (bf16[256,128]{1,0:T(8,128)(2,1)}, bf16[256,128]{1,0:T(8,128)(2,1)}, u32[]{:S(2)}, u32[]{:S(2)}) collective-permute-start(bf16[256,128]{1,0:T(8,128)(2,1)} %get-tuple-element.42), channel_id=1, source_target_pairs={{0,3},{1,7},{2,11},{3,15},{4,0},{5,4},{6,8},{7,12},{8,1},{9,5},{10... | collective-permute-start | bytes 196616 | tf_op jit(solution)/shard_map/ppermute | solution.py:137
  18.0 1.2 copy-done.1
  19.2 0.7 dynamic-slice_bitcast_fusion.31
  19.9 1.0 dynamic-slice_bitcast_fusion.8
  20.9 0.8 fusion.90
  21.9 0.7 copy-done.20
  23.3 1.3 fusion.72
  24.6 1.4 fusion.75
  26.0 1.9 collective-permute-start.12
  27.8 2.2 collective-permute-start.11
  30.1 3.0 %collective-permute-start.10 = (bf16[256,128]{1,0:T(8,128)(2,1)S(1)}, bf16[256,128]{1,0:T(8,128)(2,1)S(1)}, u32[]{:S(2)}, u32[]{:S(2)}) collective-permute-start(bf16[256,128]{1,0:T(8,128)(2,1)S(1)} %copy-done.22), channel_id=1, source_target_pairs={{0,3},{1,7},{2,11},{3,15},{4,0},{5,4},{6,8},{7,12},{8,1},{9,5},{10... | collective-permute-start | bytes 196616 | tf_op jit(solution)/shard_map/ppermute | solution.py:137
  33.7 0.9 pad_maximum_fusion.1
  34.6 6.4 %collective-permute-done.11 = bf16[256,128]{1,0:T(8,128)(2,1)S(1)} collective-permute-done((bf16[256,128]{1,0:T(8,128)(2,1)S(1)}, bf16[256,128]{1,0:T(8,128)(2,1)S(1)}, u32[]{:S(2)}, u32[]{:S(2)}) %collective-permute-start.11) | collective-permute-done | bytes 65568 | tf_op jit(solution)/shard_map/ppermute | solution.py:137
  41.2 8.6 %all_gather.18 = bf16[512,512]{1,0:T(8,128)(2,1)S(1)} all-gather(bf16[128,512]{1,0:T(8,128)(2,1)S(1)} %collective-permute-done), channel_id=1, replica_groups=mesh['grp'=2,'sp'=4,'tp'=4] {'tp'}, dimensions={0}, use_global_device_ids=true | all-gather | bytes 655360 | tf_op jit(solution)/shard_map/all_gather | solution.py:145
  49.9 1.1 collective-permute-start.7
  51.1 0.9 collective-permute-start.5
  52.0 1.0 convolution_convert_fusion.7
  53.1 1.6 collective-permute-start.1
  54.7 1.0 convolution_convert_fusion.6
  55.7 4.4 %collective-permute-start.2 = (bf16[512,256]{1,0:T(8,128)(2,1)}, bf16[512,256]{1,0:T(8,128)(2,1)S(1)}, u32[]{:S(2)}, u32[]{:S(2)}) collective-permute-start(bf16[512,256]{1,0:T(8,128)(2,1)} %convolution_convert_fusion.6), channel_id=1, source_target_pairs={{0,3},{1,7},{2,11},{3,15},{4,0},{5,4},{6,8},{7,12},{8,1},{9,5},{10... | collective-permute-start | bytes 786440 | tf_op jit(solution)/shard_map/ppermute | solution.py:137
  60.1 1.0 convolution_convert_fusion.5
  61.1 1.0 convolution_convert_fusion.4
  62.9 0.7 copy_bitcast_fusion.1.maps_ref
  63.6 0.9 copy.10.refs_4_
  64.5 5.0 %collective-permute-done.2.refs_1_ = bf16[512,256]{1,0:T(8,128)(2,1)S(1)} collective-permute-done((bf16[512,256]{1,0:T(8,128)(2,1)}, bf16[512,256]{1,0:T(8,128)(2,1)S(1)}, u32[]{:S(2)}, u32[]{:S(2)}) %collective-permute-start.2) | collective-permute-done | bytes 262176 | tf_op jit(solution)/shard_map/ppermute | solution.py:137
  69.5 29.6 %collective-permute-done.3.refs_2_ = bf16[512,256]{1,0:T(8,128)(2,1)S(1)} collective-permute-done((bf16[512,256]{1,0:T(8,128)(2,1)}, bf16[512,256]{1,0:T(8,128)(2,1)S(1)}, u32[]{:S(2)}, u32[]{:S(2)}) %collective-permute-start.3) | collective-permute-done | bytes 262176 | tf_op jit(solution)/shard_map/ppermute | solution.py:137
  99.2 0.7 copy-done.7
  100.0 2.2 conv.2
  102.2 3.6 %all_gather.19.head_ref = bf16[512,256]{1,0:T(8,128)(2,1)} all-gather(bf16[512,128]{1,0:T(8,128)(2,1)} %get-tuple-element.9.conv_ref), channel_id=1, replica_groups={{0,1},{2,3},{4,5},{6,7},{8,9},{10,11},{12,13},{14,15},{16,17},{18,19},{..., dimensions={1}, use_global_device_ids=true | all-gather | bytes 393216 | tf_op jit(solution)/shard_map/all_gather | solution.py:179
  105.8 4.2 %scan.2 = bf16[512,128]{1,0:T(8,128)(2,1)} custom-call(bf16[512,256]{1,0:T(8,128)(2,1)} %all_gather.19.head_ref, bf16[512,128]{1,0:T(8,128)(2,1)} %get-tuple-element.9.conv_ref, bf16[512,128]{1,0:T(8,128)(2,1)} %get-tuple-element.10.gin_ref, bf16[256,512]{1,0:T(8,128)(2,1)} %copy_bitcast_fusion.1.maps_ref, f32[2,128]{1,0:T(2,128)} %get-tuple-element.52.coef_ref), custom_call_target="tpu_custom_call" | custom-call | tf_op jit(solution)/shard_map/scan/pallas_call | solution.py:105
  110.0 12.5 %all_gather.20 = bf16[512,512]{1,0:T(8,128)(2,1)S(1)} all-gather(bf16[512,128]{1,0:T(8,128)(2,1)} %scan.2), channel_id=1, replica_groups=mesh['grp'=2,'sp'=4,'tp'=4] {'tp'}, dimensions={1}, use_global_device_ids=true | all-gather | bytes 655360 | tf_op jit(solution)/shard_map/all_gather | solution.py:182
  124.2 2.0 collective-permute-start.15
  126.2 1.2 collective-permute-start.14
  127.4 0.7 collective-permute-start.13
  128.3 3.8 %collective-permute-done.16 = bf16[512,128]{1,0:T(8,128)(2,1)S(1)} collective-permute-done((bf16[512,128]{1,0:T(8,128)(2,1)S(1)}, bf16[512,128]{1,0:T(8,128)(2,1)S(1)}, u32[]{:S(2)}, u32[]{:S(2)}) %collective-permute-start.16) | collective-permute-done | bytes 131104 | tf_op jit(solution)/shard_map/ppermute | solution.py:137
  132.1 12.6 %collective-permute-done.15 = bf16[512,128]{1,0:T(8,128)(2,1)S(1)} collective-permute-done((bf16[512,128]{1,0:T(8,128)(2,1)S(1)}, bf16[512,128]{1,0:T(8,128)(2,1)S(1)}, u32[]{:S(2)}, u32[]{:S(2)}) %collective-permute-start.15) | collective-permute-done | bytes 131104 | tf_op jit(solution)/shard_map/ppermute | solution.py:137
  144.8 12.7 %all_gather.21 = bf16[512,512]{1,0:T(8,128)(2,1)S(1)} all-gather(bf16[512,128]{1,0:T(8,128)(2,1)S(1)} %add_convert_fusion.1), channel_id=1, replica_groups=mesh['grp'=2,'sp'=4,'tp'=4] {'tp'}, dimensions={1}, use_global_device_ids=true | all-gather | bytes 655360 | tf_op jit(solution)/shard_map/all_gather | solution.py:193
  158.1 1.5 collective-permute-start.22
  160.1 0.7 collective-permute-start.17
  161.1 6.0 %collective-permute-start.18 = (bf16[512,256]{1,0:T(8,128)(2,1)S(1)}, bf16[512,256]{1,0:T(8,128)(2,1)S(1)}, u32[]{:S(2)}, u32[]{:S(2)}) collective-permute-start(bf16[512,256]{1,0:T(8,128)(2,1)S(1)} %convolution_convert_fusion.2), channel_id=1, source_target_pairs={{0,3},{1,7},{2,11},{3,15},{4,0},{5,4},{6,8},{7,12},{8,1},{9,5},{10... | collective-permute-start | bytes 786440 | tf_op jit(solution)/shard_map/ppermute | solution.py:137
  167.8 0.7 collective-permute-start.20
  168.5 0.7 copy_bitcast_fusion.maps_ref
  169.3 0.9 copy.12.refs_4_
  170.2 4.7 %collective-permute-done.18.refs_1_ = bf16[512,256]{1,0:T(8,128)(2,1)S(1)} collective-permute-done((bf16[512,256]{1,0:T(8,128)(2,1)S(1)}, bf16[512,256]{1,0:T(8,128)(2,1)S(1)}, u32[]{:S(2)}, u32[]{:S(2)}) %collective-permute-start.18) | collective-permute-done | bytes 262176 | tf_op jit(solution)/shard_map/ppermute | solution.py:137
  174.9 31.7 %collective-permute-done.19.refs_2_ = bf16[512,256]{1,0:T(8,128)(2,1)S(1)} collective-permute-done((bf16[512,256]{1,0:T(8,128)(2,1)S(1)}, bf16[512,256]{1,0:T(8,128)(2,1)S(1)}, u32[]{:S(2)}, u32[]{:S(2)}) %collective-permute-start.19) | collective-permute-done | bytes 262176 | tf_op jit(solution)/shard_map/ppermute | solution.py:137
  206.6 0.7 copy-done.6
  207.4 2.2 conv.3
  209.7 3.9 %all_gather.22.head_ref = bf16[512,256]{1,0:T(8,128)(2,1)} all-gather(bf16[512,128]{1,0:T(8,128)(2,1)} %get-tuple-element.11.conv_ref), channel_id=1, replica_groups={{0,1},{2,3},{4,5},{6,7},{8,9},{10,11},{12,13},{14,15},{16,17},{18,19},{..., dimensions={1}, use_global_device_ids=true | all-gather | bytes 393216 | tf_op jit(solution)/shard_map/all_gather | solution.py:179
  213.6 4.2 %scan.3 = bf16[512,128]{1,0:T(8,128)(2,1)} custom-call(bf16[512,256]{1,0:T(8,128)(2,1)} %all_gather.22.head_ref, bf16[512,128]{1,0:T(8,128)(2,1)} %get-tuple-element.11.conv_ref, bf16[512,128]{1,0:T(8,128)(2,1)} %get-tuple-element.12.gin_ref, bf16[256,512]{1,0:T(8,128)(2,1)} %copy_bitcast_fusion.maps_ref, f32[2,128]{1,0:T(2,128)} %get-tuple-element.51.coef_ref), custom_call_target="tpu_custom_call" | custom-call | tf_op jit(solution)/shard_map/scan/pallas_call | solution.py:105
  217.8 12.5 %all_gather.23 = bf16[512,512]{1,0:T(8,128)(2,1)S(1)} all-gather(bf16[512,128]{1,0:T(8,128)(2,1)} %scan.3), channel_id=1, replica_groups=mesh['grp'=2,'sp'=4,'tp'=4] {'tp'}, dimensions={1}, use_global_device_ids=true | all-gather | bytes 655360 | tf_op jit(solution)/shard_map/all_gather | solution.py:182
  230.6 1.6 collective-permute-start.30
  233.9 2.6 %collective-permute-done.30 = bf16[128,512]{1,0:T(8,128)(2,1)S(1)} collective-permute-done((bf16[128,512]{1,0:T(8,128)(2,1)S(1)}, bf16[128,512]{1,0:T(8,128)(2,1)S(1)}, u32[]{:S(2)}, u32[]{:S(2)}) %collective-permute-start.30) | collective-permute-done | bytes 131104 | tf_op jit(solution)/shard_map/ppermute | solution.py:202
  236.5 8.4 %collective-permute-done.29 = bf16[128,512]{1,0:T(8,128)(2,1)S(1)} collective-permute-done((bf16[128,512]{1,0:T(8,128)(2,1)S(1)}, bf16[128,512]{1,0:T(8,128)(2,1)S(1)}, u32[]{:S(2)}, u32[]{:S(2)}) %collective-permute-start.29) | collective-permute-done | bytes 131104 | tf_op jit(solution)/shard_map/ppermute | solution.py:202
  245.3 0.8 collective-permute-start.33
  246.1 0.7 collective-permute-start.32
  247.4 2.3 collective-permute-done.32
  249.9 0.8 fusion.25
  (108 shorter events, 9.8 us)
Async XLA Ops:
  0.0 17.9 %copy-start = (bf16[2,512,512]{2,1,0:T(8,128)(2,1)S(1)}, bf16[2,512,512]{2,1,0:T(8,128)(2,1)}, u32[]{:S(2)}) copy-start(bf16[2,512,512]{2,1,0:T(8,128)(2,1)} %param.12) | copy-start | bytes 3145732
  0.0 41.1 %collective-permute-start = (bf16[128,512]{1,0:T(8,128)(2,1)}, bf16[128,512]{1,0:T(8,128)(2,1)S(1)}, u32[]{:S(2)}, u32[]{:S(2)}) collective-permute-start(bf16[128,512]{1,0:T(8,128)(2,1)} %param.9), channel_id=1, source_target_pairs={{0,0},{1,4},{2,8},{3,12},{4,1},{5,5},{6,9},{7,13},{8,2},{9,6},{10,... | collective-permute-start | bytes 393224 | tf_op jit(solution)/shard_map/ppermute | solution.py:142
  3.0 18.9 %collective-permute-start.8 = (f32[2,6,512]{2,1,0:T(8,128)}, f32[2,6,512]{2,1,0:T(8,128)}, u32[]{:S(2)}, u32[]{:S(2)}) collective-permute-start(f32[2,6,512]{2,1,0:T(8,128)} %pad_maximum_fusion.2), channel_id=1, source_target_pairs={{0,0},{1,4},{2,8},{3,12},{4,1},{5,5},{6,9},{7,13},{8,2},{9,6},{10,... | collective-permute-start | bytes 73736 | tf_op jit(solution)/shard_map/ppermute | solution.py:144
  6.9 19.0 %collective-permute-start.27 = (bf16[256,128]{1,0:T(8,128)(2,1)}, bf16[256,128]{1,0:T(8,128)(2,1)}, u32[]{:S(2)}, u32[]{:S(2)}) collective-permute-start(bf16[256,128]{1,0:T(8,128)(2,1)} %get-tuple-element.40), channel_id=1, source_target_pairs={{0,1},{1,5},{2,9},{3,13},{4,2},{5,6},{6,10},{7,14},{8,3},{9,7},{10... | collective-permute-start | bytes 196616 | tf_op jit(solution)/shard_map/ppermute | solution.py:137
  10.5 17.3 %collective-permute-start.26 = (bf16[256,128]{1,0:T(8,128)(2,1)}, bf16[256,128]{1,0:T(8,128)(2,1)}, u32[]{:S(2)}, u32[]{:S(2)}) collective-permute-start(bf16[256,128]{1,0:T(8,128)(2,1)} %get-tuple-element.41), channel_id=1, source_target_pairs={{0,2},{1,6},{2,10},{3,14},{4,3},{5,7},{6,11},{7,15},{8,0},{9,4},{1... | collective-permute-start | bytes 196616 | tf_op jit(solution)/shard_map/ppermute | solution.py:137
  15.0 15.1 %collective-permute-start.25 = (bf16[256,128]{1,0:T(8,128)(2,1)}, bf16[256,128]{1,0:T(8,128)(2,1)}, u32[]{:S(2)}, u32[]{:S(2)}) collective-permute-start(bf16[256,128]{1,0:T(8,128)(2,1)} %get-tuple-element.42), channel_id=1, source_target_pairs={{0,3},{1,7},{2,11},{3,15},{4,0},{5,4},{6,8},{7,12},{8,1},{9,5},{10... | collective-permute-start | bytes 196616 | tf_op jit(solution)/shard_map/ppermute | solution.py:137
  17.9 1.2 copy-start.1
  19.9 1.8 copy-start.10
  21.8 0.8 copy-start.20
  21.8 4.1 %copy-start.24 = (bf16[256,128]{1,0:T(8,128)(2,1)S(1)}, bf16[256,128]{1,0:T(8,128)(2,1)}, u32[]{:S(2)}) copy-start(bf16[256,128]{1,0:T(8,128)(2,1)} %get-tuple-element.48) | copy-start | bytes 196612
  21.8 6.0 %copy-start.23 = (bf16[256,128]{1,0:T(8,128)(2,1)S(1)}, bf16[256,128]{1,0:T(8,128)(2,1)}, u32[]{:S(2)}) copy-start(bf16[256,128]{1,0:T(8,128)(2,1)} %get-tuple-element.49) | copy-start | bytes 196612
  21.8 8.2 %copy-start.22 = (bf16[256,128]{1,0:T(8,128)(2,1)S(1)}, bf16[256,128]{1,0:T(8,128)(2,1)}, u32[]{:S(2)}) copy-start(bf16[256,128]{1,0:T(8,128)(2,1)} %get-tuple-element.50) | copy-start | bytes 196612
  21.8 11.2 %copy-start.21 = (bf16[256,128]{1,0:T(8,128)(2,1)S(1)}, bf16[256,128]{1,0:T(8,128)(2,1)}, u32[]{:S(2)}) copy-start(bf16[256,128]{1,0:T(8,128)(2,1)} %get-tuple-element.47) | copy-start | bytes 196612
  22.6 10.4 %collective-permute-start.24 = (bf16[256,128]{1,0:T(8,128)(2,1)S(1)}, bf16[256,128]{1,0:T(8,128)(2,1)S(1)}, u32[]{:S(2)}, u32[]{:S(2)}) collective-permute-start(bf16[256,128]{1,0:T(8,128)(2,1)S(1)} %copy-done.20), channel_id=1, source_target_pairs={{0,0},{1,4},{2,8},{3,12},{4,1},{5,5},{6,9},{7,13},{8,2},{9,6},{10,... | collective-permute-start | bytes 196616 | tf_op jit(solution)/shard_map/ppermute | solution.py:137
  26.0 8.7 %collective-permute-start.12 = (bf16[256,128]{1,0:T(8,128)(2,1)S(1)}, bf16[256,128]{1,0:T(8,128)(2,1)S(1)}, u32[]{:S(2)}, u32[]{:S(2)}) collective-permute-start(bf16[256,128]{1,0:T(8,128)(2,1)S(1)} %copy-done.24), channel_id=1, source_target_pairs={{0,1},{1,5},{2,9},{3,13},{4,2},{5,6},{6,10},{7,14},{8,3},{9,7},{10... | collective-permute-start | bytes 196616 | tf_op jit(solution)/shard_map/ppermute | solution.py:137
  27.8 13.2 %collective-permute-start.11 = (bf16[256,128]{1,0:T(8,128)(2,1)S(1)}, bf16[256,128]{1,0:T(8,128)(2,1)S(1)}, u32[]{:S(2)}, u32[]{:S(2)}) collective-permute-start(bf16[256,128]{1,0:T(8,128)(2,1)S(1)} %copy-done.23), channel_id=1, source_target_pairs={{0,2},{1,6},{2,10},{3,14},{4,3},{5,7},{6,11},{7,15},{8,0},{9,4},{1... | collective-permute-start | bytes 196616 | tf_op jit(solution)/shard_map/ppermute | solution.py:137
  30.1 11.0 %collective-permute-start.10 = (bf16[256,128]{1,0:T(8,128)(2,1)S(1)}, bf16[256,128]{1,0:T(8,128)(2,1)S(1)}, u32[]{:S(2)}, u32[]{:S(2)}) collective-permute-start(bf16[256,128]{1,0:T(8,128)(2,1)S(1)} %copy-done.22), channel_id=1, source_target_pairs={{0,3},{1,7},{2,11},{3,15},{4,0},{5,4},{6,8},{7,12},{8,1},{9,5},{10... | collective-permute-start | bytes 196616 | tf_op jit(solution)/shard_map/ppermute | solution.py:137
  33.0 8.0 %collective-permute-start.9 = (bf16[256,128]{1,0:T(8,128)(2,1)S(1)}, bf16[256,128]{1,0:T(8,128)(2,1)S(1)}, u32[]{:S(2)}, u32[]{:S(2)}) collective-permute-start(bf16[256,128]{1,0:T(8,128)(2,1)S(1)} %copy-done.21), channel_id=1, source_target_pairs={{0,0},{1,4},{2,8},{3,12},{4,1},{5,5},{6,9},{7,13},{8,2},{9,6},{10,... | collective-permute-start | bytes 196616 | tf_op jit(solution)/shard_map/ppermute | solution.py:137
  49.7 2.3 copy-start.18
  49.8 2.3 copy-start.19
  49.9 12.2 %collective-permute-start.7 = (f32[512]{0:T(512)S(1)}, f32[512]{0:T(512)S(1)}, u32[]{:S(2)}, u32[]{:S(2)}) collective-permute-start(f32[512]{0:T(512)S(1)} %fusion.4), channel_id=1, source_target_pairs={{0,12},{4,0},{8,4},{12,8},{1,13},{5,1},{9,5},{13,9},{2,14},{6,2},{... | collective-permute-start | bytes 6152 | tf_op jit(solution)/shard_map/ppermute | solution.py:166
  51.1 11.5 %collective-permute-start.6 = (f32[512]{0:T(512)S(1)}, f32[512]{0:T(512)S(1)}, u32[]{:S(2)}, u32[]{:S(2)}) collective-permute-start(f32[512]{0:T(512)S(1)} %fusion.4), channel_id=1, source_target_pairs={{0,8},{4,12},{8,0},{12,4},{1,9},{5,13},{9,1},{13,5},{2,10},{6,14},... | collective-permute-start | bytes 6152 | tf_op jit(solution)/shard_map/ppermute | solution.py:166
  51.1 12.6 %collective-permute-start.5 = (f32[512]{0:T(512)S(1)}, f32[512]{0:T(512)S(1)}, u32[]{:S(2)}, u32[]{:S(2)}) collective-permute-start(f32[512]{0:T(512)S(1)} %fusion.4), channel_id=1, source_target_pairs={{0,4},{4,8},{8,12},{12,0},{1,5},{5,9},{9,13},{13,1},{2,6},{6,10},{... | collective-permute-start | bytes 6152 | tf_op jit(solution)/shard_map/ppermute | solution.py:166
  52.0 2.6 %copy-start.16 = (bf16[512,128]{1,0:T(8,128)(2,1)S(1)}, bf16[512,128]{1,0:T(8,128)(2,1)}, u32[]{:S(2)}) copy-start(bf16[512,128]{1,0:T(8,128)(2,1)} %get-tuple-element.33) | copy-start | bytes 393220
  52.0 2.6 %copy-start.17 = (bf16[512,128]{1,0:T(8,128)(2,1)S(1)}, bf16[512,128]{1,0:T(8,128)(2,1)}, u32[]{:S(2)}) copy-start(bf16[512,128]{1,0:T(8,128)(2,1)} %get-tuple-element.64) | copy-start | bytes 393220
  53.1 11.4 %collective-permute-start.1 = (bf16[512,256]{1,0:T(8,128)(2,1)}, bf16[512,256]{1,0:T(8,128)(2,1)S(1)}, u32[]{:S(2)}, u32[]{:S(2)}) collective-permute-start(bf16[512,256]{1,0:T(8,128)(2,1)} %convolution_convert_fusion.7), channel_id=1, source_target_pairs={{0,0},{1,4},{2,8},{3,12},{4,1},{5,5},{6,9},{7,13},{8,2},{9,6},{10,... | collective-permute-start | bytes 786440 | tf_op jit(solution)/shard_map/ppermute | solution.py:137
  54.7 5.4 %copy-start.14 = (bf16[512,128]{1,0:T(8,128)(2,1)S(1)}, bf16[512,128]{1,0:T(8,128)(2,1)}, u32[]{:S(2)}) copy-start(bf16[512,128]{1,0:T(8,128)(2,1)} %get-tuple-element.32) | copy-start | bytes 393220
  54.7 5.4 %copy-start.15 = (bf16[512,128]{1,0:T(8,128)(2,1)S(1)}, bf16[512,128]{1,0:T(8,128)(2,1)}, u32[]{:S(2)}) copy-start(bf16[512,128]{1,0:T(8,128)(2,1)} %get-tuple-element.65) | copy-start | bytes 393220
  55.7 13.9 %collective-permute-start.2 = (bf16[512,256]{1,0:T(8,128)(2,1)}, bf16[512,256]{1,0:T(8,128)(2,1)S(1)}, u32[]{:S(2)}, u32[]{:S(2)}) collective-permute-start(bf16[512,256]{1,0:T(8,128)(2,1)} %convolution_convert_fusion.6), channel_id=1, source_target_pairs={{0,3},{1,7},{2,11},{3,15},{4,0},{5,4},{6,8},{7,12},{8,1},{9,5},{10... | collective-permute-start | bytes 786440 | tf_op jit(solution)/shard_map/ppermute | solution.py:137
  60.1 1.1 copy-start.12
  60.1 1.1 copy-start.13
  62.2 37.0 %collective-permute-start.3 = (bf16[512,256]{1,0:T(8,128)(2,1)}, bf16[512,256]{1,0:T(8,128)(2,1)S(1)}, u32[]{:S(2)}, u32[]{:S(2)}) collective-permute-start(bf16[512,256]{1,0:T(8,128)(2,1)} %convolution_convert_fusion.5), channel_id=1, source_target_pairs={{0,2},{1,6},{2,10},{3,14},{4,3},{5,7},{6,11},{7,15},{8,0},{9,4},{1... | collective-permute-start | bytes 786440 | tf_op jit(solution)/shard_map/ppermute | solution.py:137
  62.5 36.7 %collective-permute-start.4 = (bf16[512,256]{1,0:T(8,128)(2,1)}, bf16[512,256]{1,0:T(8,128)(2,1)S(1)}, u32[]{:S(2)}, u32[]{:S(2)}) collective-permute-start(bf16[512,256]{1,0:T(8,128)(2,1)} %convolution_convert_fusion.4), channel_id=1, source_target_pairs={{0,1},{1,5},{2,9},{3,13},{4,2},{5,6},{6,10},{7,14},{8,3},{9,7},{10... | collective-permute-start | bytes 786440 | tf_op jit(solution)/shard_map/ppermute | solution.py:137
  64.5 34.7 %copy-start.3 = (bf16[512,256]{1,0:T(8,128)(2,1)}, bf16[512,256]{1,0:T(8,128)(2,1)S(1)}, u32[]{:S(2)}) copy-start(bf16[512,256]{1,0:T(8,128)(2,1)S(1)} %collective-permute-done.1.refs_0_) | copy-start | bytes 786436
  69.5 29.7 %copy-start.5 = (bf16[512,256]{1,0:T(8,128)(2,1)}, bf16[512,256]{1,0:T(8,128)(2,1)S(1)}, u32[]{:S(2)}) copy-start(bf16[512,256]{1,0:T(8,128)(2,1)S(1)} %collective-permute-done.2.refs_1_) | copy-start | bytes 786436
  99.2 0.7 copy-start.7
  99.2 0.8 copy-start.9
  123.8 8.3 %collective-permute-start.16 = (bf16[512,128]{1,0:T(8,128)(2,1)S(1)}, bf16[512,128]{1,0:T(8,128)(2,1)S(1)}, u32[]{:S(2)}, u32[]{:S(2)}) collective-permute-start(bf16[512,128]{1,0:T(8,128)(2,1)S(1)} %convolution_convert_fusion.8), channel_id=1, source_target_pairs={{0,1},{1,5},{2,9},{3,13},{4,2},{5,6},{6,10},{7,14},{8,3},{9,7},{10... | collective-permute-start | bytes 393224 | tf_op jit(solution)/shard_map/ppermute | solution.py:137
  124.2 20.5 %collective-permute-start.15 = (bf16[512,128]{1,0:T(8,128)(2,1)S(1)}, bf16[512,128]{1,0:T(8,128)(2,1)S(1)}, u32[]{:S(2)}, u32[]{:S(2)}) collective-permute-start(bf16[512,128]{1,0:T(8,128)(2,1)S(1)} %convolution_convert_fusion.9), channel_id=1, source_target_pairs={{0,2},{1,6},{2,10},{3,14},{4,3},{5,7},{6,11},{7,15},{8,0},{9,4},{1... | collective-permute-start | bytes 393224 | tf_op jit(solution)/shard_map/ppermute | solution.py:137
  126.2 18.5 %collective-permute-start.14 = (bf16[512,128]{1,0:T(8,128)(2,1)S(1)}, bf16[512,128]{1,0:T(8,128)(2,1)S(1)}, u32[]{:S(2)}, u32[]{:S(2)}) collective-permute-start(bf16[512,128]{1,0:T(8,128)(2,1)S(1)} %convolution_convert_fusion.10), channel_id=1, source_target_pairs={{0,3},{1,7},{2,11},{3,15},{4,0},{5,4},{6,8},{7,12},{8,1},{9,5},{10... | collective-permute-start | bytes 393224 | tf_op jit(solution)/shard_map/ppermute | solution.py:137
  127.4 17.3 %collective-permute-start.13 = (bf16[512,128]{1,0:T(8,128)(2,1)S(1)}, bf16[512,128]{1,0:T(8,128)(2,1)S(1)}, u32[]{:S(2)}, u32[]{:S(2)}) collective-permute-start(bf16[512,128]{1,0:T(8,128)(2,1)S(1)} %convolution_convert_fusion.11), channel_id=1, source_target_pairs={{0,0},{1,4},{2,8},{3,12},{4,1},{5,5},{6,9},{7,13},{8,2},{9,6},{10,... | collective-permute-start | bytes 393224 | tf_op jit(solution)/shard_map/ppermute | solution.py:137
  157.7 10.1 %collective-permute-start.23 = (f32[512]{0:T(512)S(1)}, f32[512]{0:T(512)S(1)}, u32[]{:S(2)}, u32[]{:S(2)}) collective-permute-start(f32[512]{0:T(512)S(1)} %fusion.6), channel_id=1, source_target_pairs={{0,12},{4,0},{8,4},{12,8},{1,13},{5,1},{9,5},{13,9},{2,14},{6,2},{... | collective-permute-start | bytes 6152 | tf_op jit(solution)/shard_map/ppermute | solution.py:166
  158.1 9.8 %collective-permute-start.22 = (f32[512]{0:T(512)S(1)}, f32[512]{0:T(512)S(1)}, u32[]{:S(2)}, u32[]{:S(2)}) collective-permute-start(f32[512]{0:T(512)S(1)} %fusion.6), channel_id=1, source_target_pairs={{0,8},{4,12},{8,0},{12,4},{1,9},{5,13},{9,1},{13,5},{2,10},{6,14},... | collective-permute-start | bytes 6152 | tf_op jit(solution)/shard_map/ppermute | solution.py:166
  159.5 9.8 %collective-permute-start.21 = (f32[512]{0:T(512)S(1)}, f32[512]{0:T(512)S(1)}, u32[]{:S(2)}, u32[]{:S(2)}) collective-permute-start(f32[512]{0:T(512)S(1)} %fusion.6), channel_id=1, source_target_pairs={{0,4},{4,8},{8,12},{12,0},{1,5},{5,9},{9,13},{13,1},{2,6},{6,10},{... | collective-permute-start | bytes 6152 | tf_op jit(solution)/shard_map/ppermute | solution.py:166
  160.1 10.1 %collective-permute-start.17 = (bf16[512,256]{1,0:T(8,128)(2,1)S(1)}, bf16[512,256]{1,0:T(8,128)(2,1)S(1)}, u32[]{:S(2)}, u32[]{:S(2)}) collective-permute-start(bf16[512,256]{1,0:T(8,128)(2,1)S(1)} %convolution_convert_fusion.3), channel_id=1, source_target_pairs={{0,0},{1,4},{2,8},{3,12},{4,1},{5,5},{6,9},{7,13},{8,2},{9,6},{10,... | collective-permute-start | bytes 786440 | tf_op jit(solution)/shard_map/ppermute | solution.py:137
  161.1 13.8 %collective-permute-start.18 = (bf16[512,256]{1,0:T(8,128)(2,1)S(1)}, bf16[512,256]{1,0:T(8,128)(2,1)S(1)}, u32[]{:S(2)}, u32[]{:S(2)}) collective-permute-start(bf16[512,256]{1,0:T(8,128)(2,1)S(1)} %convolution_convert_fusion.2), channel_id=1, source_target_pairs={{0,3},{1,7},{2,11},{3,15},{4,0},{5,4},{6,8},{7,12},{8,1},{9,5},{10... | collective-permute-start | bytes 786440 | tf_op jit(solution)/shard_map/ppermute | solution.py:137
  167.8 38.8 %collective-permute-start.19 = (bf16[512,256]{1,0:T(8,128)(2,1)S(1)}, bf16[512,256]{1,0:T(8,128)(2,1)S(1)}, u32[]{:S(2)}, u32[]{:S(2)}) collective-permute-start(bf16[512,256]{1,0:T(8,128)(2,1)S(1)} %convolution_convert_fusion.1), channel_id=1, source_target_pairs={{0,2},{1,6},{2,10},{3,14},{4,3},{5,7},{6,11},{7,15},{8,0},{9,4},{1... | collective-permute-start | bytes 786440 | tf_op jit(solution)/shard_map/ppermute | solution.py:137
  167.8 38.7 %collective-permute-start.20 = (bf16[512,256]{1,0:T(8,128)(2,1)S(1)}, bf16[512,256]{1,0:T(8,128)(2,1)S(1)}, u32[]{:S(2)}, u32[]{:S(2)}) collective-permute-start(bf16[512,256]{1,0:T(8,128)(2,1)S(1)} %convolution_convert_fusion), channel_id=1, source_target_pairs={{0,1},{1,5},{2,9},{3,13},{4,2},{5,6},{6,10},{7,14},{8,3},{9,7},{10... | collective-permute-start | bytes 786440 | tf_op jit(solution)/shard_map/ppermute | solution.py:137
  170.2 36.4 %copy-start.2 = (bf16[512,256]{1,0:T(8,128)(2,1)}, bf16[512,256]{1,0:T(8,128)(2,1)S(1)}, u32[]{:S(2)}) copy-start(bf16[512,256]{1,0:T(8,128)(2,1)S(1)} %collective-permute-done.17.refs_0_) | copy-start | bytes 786436
  174.9 31.7 %copy-start.4 = (bf16[512,256]{1,0:T(8,128)(2,1)}, bf16[512,256]{1,0:T(8,128)(2,1)S(1)}, u32[]{:S(2)}) copy-start(bf16[512,256]{1,0:T(8,128)(2,1)S(1)} %collective-permute-done.18.refs_1_) | copy-start | bytes 786436
  206.6 0.7 copy-start.6
  206.6 0.8 copy-start.8
  209.7 20.7 %copy-start.11 = (bf16[2,512,512]{2,1,0:T(8,128)(2,1)S(1)}, bf16[2,512,512]{2,1,0:T(8,128)(2,1)}, u32[]{:S(2)}) copy-start(bf16[2,512,512]{2,1,0:T(8,128)(2,1)} %param.16) | copy-start | bytes 3145732
  230.6 5.9 %collective-permute-start.30 = (bf16[128,512]{1,0:T(8,128)(2,1)S(1)}, bf16[128,512]{1,0:T(8,128)(2,1)S(1)}, u32[]{:S(2)}, u32[]{:S(2)}) collective-permute-start(bf16[128,512]{1,0:T(8,128)(2,1)S(1)} %fusion.2), channel_id=1, source_target_pairs={{0,12},{4,0},{8,4},{12,8},{1,13},{5,1},{9,5},{13,9},{2,14},{6,2},{... | collective-permute-start | bytes 393224 | tf_op jit(solution)/shard_map/ppermute | solution.py:202
  232.4 12.5 %collective-permute-start.29 = (bf16[128,512]{1,0:T(8,128)(2,1)S(1)}, bf16[128,512]{1,0:T(8,128)(2,1)S(1)}, u32[]{:S(2)}, u32[]{:S(2)}) collective-permute-start(bf16[128,512]{1,0:T(8,128)(2,1)S(1)} %fusion.1), channel_id=1, source_target_pairs={{0,8},{4,12},{8,0},{12,4},{1,9},{5,13},{9,1},{13,5},{2,10},{6,14},... | collective-permute-start | bytes 393224 | tf_op jit(solution)/shard_map/ppermute | solution.py:202
  233.3 11.6 %collective-permute-start.28 = (bf16[128,512]{1,0:T(8,128)(2,1)S(1)}, bf16[128,512]{1,0:T(8,128)(2,1)S(1)}, u32[]{:S(2)}, u32[]{:S(2)}) collective-permute-start(bf16[128,512]{1,0:T(8,128)(2,1)S(1)} %fusion), channel_id=1, source_target_pairs={{0,4},{4,8},{8,12},{12,0},{1,5},{5,9},{9,13},{13,1},{2,6},{6,10},{... | collective-permute-start | bytes 393224 | tf_op jit(solution)/shard_map/ppermute | solution.py:202
  245.3 4.6 %copy-start.25 = (f32[512]{0:T(512)S(1)}, f32[512]{0:T(512)}, u32[]{:S(2)}) copy-start(f32[512]{0:T(512)} %param.17) | copy-start | bytes 6148
  245.3 2.1 collective-permute-start.33
  246.1 3.6 %collective-permute-start.32 = (f32[128]{0:T(128)S(1)}, f32[128]{0:T(128)S(1)}, u32[]{:S(2)}, u32[]{:S(2)}) collective-permute-start(f32[128]{0:T(128)S(1)} %get-tuple-element.57), channel_id=1, source_target_pairs={{0,2},{1,3},{2,0},{3,1},{4,6},{5,7},{6,4},{7,5},{8,10},{9,11},{10,... | collective-permute-start | bytes 1544 | tf_op jit(solution)/shard_map/ppermute | solution.py:211
  246.9 3.0 %collective-permute-start.31 = (f32[128]{0:T(128)S(1)}, f32[128]{0:T(128)S(1)}, u32[]{:S(2)}, u32[]{:S(2)}) collective-permute-start(f32[128]{0:T(128)S(1)} %get-tuple-element.57), channel_id=1, source_target_pairs={{0,1},{1,2},{2,3},{3,0},{4,5},{5,6},{6,7},{7,4},{8,9},{9,10},{10,1... | collective-permute-start | bytes 1544 | tf_op jit(solution)/shard_map/ppermute | solution.py:211

commit v2 on v1

--- a/solution.py
+++ b/solution.py
@@ -17,15 +17,13 @@
 
 
 def conv_kernel(*refs):
-    pieces = refs[:-4]
-    scale_ref, taps_ref, conv_ref, gin_ref = refs[-4:]
+    pieces = refs[:-3]
+    scale_ref, taps_ref, conv_ref = refs[-3:]
     total = pieces[0][...].astype(F32)
     for piece in pieces[1:]:
         total = total + piece[...].astype(F32)
-    total = total * scale_ref[...]
     length, width = conv_ref.shape
-    gin_ref[...] = total[:, width:].astype(BF)
-    xin = total[:, :width].astype(BF).astype(F32)
+    xin = (total * scale_ref[...]).astype(BF).astype(F32)
     row = lax.broadcasted_iota(jnp.int32, (length, width), 0)
     conv = None
     for k in range(TAPS):
@@ -47,7 +45,7 @@
     return jnp.where(y > -0.5, -y * series, 1.0 - jnp.exp(y))
 
 
-def scan_kernel(head_ref, conv_ref, gin_ref, maps_ref, coef_ref, mix_ref, a0, b0, a1, b1):
+def scan_kernel(head_ref, conv_ref, maps_ref, coef_ref, hidden_ref, a0, b0, a1, b1):
     length, width = conv_ref.shape
     steps = length // SEGS
     conv = conv_ref[...].astype(F32)
@@ -90,24 +88,24 @@
         carry = pb[s : s + 1] * carry + hb[s : s + 1]
     for s in range(SEGS):
         rows = slice(s * steps, (s + 1) * steps)
-        hidden = b0[rows, :] + a0[rows, :] * fwd[s] + b1[rows, :] + a1[rows, :] * bwd[s]
-        gate = jax.nn.gelu(gin_ref[rows, :].astype(F32), approximate=True)
-        mix_ref[rows, :] = (gate * hidden).astype(BF)
+        hidden_ref[rows, :] = (
+            b0[rows, :] + a0[rows, :] * fwd[s] + b1[rows, :] + a1[rows, :] * bwd[s]
+        )
 
 
 def conv_call(pieces, scale, taps):
     length, width = pieces[0].shape[0], taps.shape[1]
     out = jax.ShapeDtypeStruct((length, width), BF)
-    return pl.pallas_call(conv_kernel, out_shape=(out, out), name="conv")(*pieces, scale, taps)
-
-
-def scan_call(head, conv, gin, maps, coef):
+    return pl.pallas_call(conv_kernel, out_shape=out, name="conv")(*pieces, scale, taps)
+
+
+def scan_call(head, conv, maps, coef):
     return pl.pallas_call(
         scan_kernel,
-        out_shape=jax.ShapeDtypeStruct(conv.shape, BF),
+        out_shape=jax.ShapeDtypeStruct(conv.shape, F32),
         scratch_shapes=[pltpu.VMEM(conv.shape, F32)] * 4,
         name="scan",
-    )(head, conv, gin, maps, coef)
+    )(head, conv, maps, coef)
 
 
 def body_square(
@@ -136,27 +134,53 @@
     def scatter(make):
         return [lax.ppermute(make((s - k) % n), axes, to_piece[k]) for k in range(n)]
 
+    half = n // 2
+    flip = [(b, (b + half) % n) for b in range(n)]
+    side = q // half
+    by_side = [[] for _ in range(n)]
+    for k in range(n):
+        for a in range(n):
+            for b in range(n):
+                kind, core = ((a ^ k) % 2, (a ^ k) // 2)
+                dest = (b + kind * half) % n
+                by_side[k].append((a * n + b, dest * n + b // half * half + core))
+
+    def scatter_sides(make):
+        other = jnp.stack([make((1 - side) * half + c) for c in range(half)])
+        passed = lax.ppermute(other, "tp", flip)
+        held = jnp.stack([v for c in range(half) for v in (make(side * half + c), passed[c])])
+        return [lax.dynamic_index_in_dim(held, s ^ k, 0, False) for k in range(n)]
+
+    def gather_cols(value, sets=None):
+        got = lax.all_gather(value, "tp", axis=0, axis_index_groups=sets)
+        return jnp.concatenate([got[i] for i in range(got.shape[0])], axis=1)
+
     def cols(value, at, size):
         return lax.dynamic_slice_in_dim(value, at * size, size, value.ndim - 1)
 
     turned = lax.ppermute(tokens, axes, swap)
+    gain = cols(norm_gain, s, block)
+
+    def cuts_of(held):
+        def cut(piece):
+            at = (piece // group * HEAD_W, piece % group * width)
+            return lax.dynamic_slice(held, at, (HEAD_W, width))
+
+        return [cut((s - k) % n) for k in range(n)]
+
+    def maps_of(cuts):
+        got = [lax.ppermute(cuts[k], axes, to_piece[k]) for k in range(n)]
+        ordered = jnp.stack(got)
+        ordered = jnp.stack([lax.dynamic_index_in_dim(ordered, (g - q) % n, 0, False) for g in range(n)], 1)
+        return ordered.reshape(HEAD_W, n * width)
+
     small = jnp.concatenate([conv_taps, decay_logit], axis=1)
+    cuts = cuts_of(gate_maps[0])
+    small, cuts, turned = lax.optimization_barrier((small, cuts, turned))
+    maps = maps_of(cuts)
     small = cols(lax.ppermute(small, axes, swap), q, width)
     full = lax.all_gather(turned, "tp", axis=0, tiled=True)
     own = cols(full, q, width)
-    gain = cols(norm_gain, s, block)
-
-    def maps_of(layer):
-        held = gate_maps[layer]
-
-        def cut(piece):
-            at = (piece // group * HEAD_W, piece % group * width)
-            return lax.dynamic_slice(held, at, (HEAD_W, width))
-
-        got = scatter(cut)
-        ordered = jnp.stack(got)
-        ordered = jnp.stack([lax.dynamic_index_in_dim(ordered, (g - q) % n, 0, False) for g in range(n)], 1)
-        return ordered.reshape(HEAD_W, n * width)
 
     for layer in range(LAYERS):
         wide = full.astype(F32)
@@ -167,19 +191,33 @@
         scale = lax.rsqrt(total / D + EPS)[:, None]
         scaled = (wide * gain[layer]).astype(BF)
 
-        def project(piece):
-            w = jnp.concatenate(
-                [cols(in_weight[layer], piece, width), cols(gate_weight[layer], piece, width)], axis=1
-            )
-            return jnp.dot(scaled, w, preferred_element_type=F32).astype(BF)
-
-        conv, gin = conv_call(scatter(project), scale, small[layer, :TAPS])
-        head = conv
-        if group > 1:
-            head = lax.all_gather(conv, "tp", axis=1, tiled=True, axis_index_groups=sets)
+        def project(weight, value):
+            return lambda piece: jnp.dot(
+                value, cols(weight, piece, width), preferred_element_type=F32
+            ).astype(BF)
+
+        xparts = [project(in_weight[layer], scaled)((s - k) % n) for k in range(n)]
+        xparts, scaled = lax.optimization_barrier((xparts, scaled))
+        conv = conv_call(
+            [lax.ppermute(xparts[k], axes, to_piece[k]) for k in range(n)],
+            scale,
+            small[layer, :TAPS],
+        )
+        gins = scatter_sides(project(gate_weight[layer], scaled))
+        gins, conv = lax.optimization_barrier((gins, conv))
+        gins = [lax.ppermute(gins[k], axes, by_side[k]) for k in range(n)]
+        head = gather_cols(conv, sets) if group > 1 else conv
         coef = -8.0 * jax.nn.softplus(-small[layer, TAPS:])
-        mix = scan_call(head, conv, gin, maps_of(layer), coef)
-        mixed = lax.all_gather(mix, "tp", axis=1, tiled=True)
+        hidden = scan_call(head, conv, maps, coef)
+        gin = gins[0].astype(F32)
+        for piece in gins[1:]:
+            gin = gin + piece.astype(F32)
+        gin = (gin * scale).astype(BF).astype(F32)
+        mix = (jax.nn.gelu(gin, approximate=True) * hidden).astype(BF)
+        if layer + 1 < LAYERS:
+            cuts, mix = lax.optimization_barrier((cuts_of(gate_maps[layer + 1]), mix))
+            maps = maps_of(cuts)
+        mixed = gather_cols(mix)
         if layer + 1 < LAYERS:
             pieces = scatter(
                 lambda piece: jnp.dot(
@@ -190,7 +228,7 @@
             for piece in pieces:
                 out = out + piece.astype(F32)
             own = out.astype(BF)
-            full = lax.all_gather(own, "tp", axis=1, tiled=True)
+            full = gather_cols(own)
         else:
             here = (s == q).astype(F32)
 

time: 251 us -> 240 us (0.956)
  waiting for transfers between devices: 108 us -> 65.9 us
  starting transfers between devices: 50.1 us -> 83.6 us
  blocking collectives: 53.9 us -> 41.9 us
  local copies, waits for them, and re-layouts: 11.3 us -> 14.5 us
  other arithmetic: 6.4 us -> 9.12 us
    ppermute x20 -> x4, waiting for transfers between devices: 94 us -> 14.6 us  [scatter(): lax.ppermute(make((s - k) % n), axes, to_piece[k])]
    ppermute x0 -> x26, starting transfers between devices: none -> 56.5 us  [the longest x8 22 us: body_square(): gins = [lax.ppermute(gins[k], axes, by_side[k]) for k in range(n)]]
    ppermute x0 -> x26, waiting for transfers between devices: none -> 41 us  [the longest x8 33.8 us: body_square(): lax.ppermute(xparts[k], axes, to_piece[k])]
    ppermute x20 -> x4, starting transfers between devices: 37.7 us -> 10.2 us  [scatter(): lax.ppermute(make((s - k) % n), axes, to_piece[k])]
    all_gather x5, blocking collectives: 45.3 us -> 29.5 us  [gather_cols(): got = lax.all_gather(value, 'tp', axis=0, axis_index_groups=sets)]
    ppermute x6, starting transfers between devices: 4.16 us -> 8.25 us  [body_square(): total = total + lax.ppermute(part, 'sp', rotate[k])]
    all_gather x1, blocking collectives: 8.59 us -> 12.4 us  [body_square(): full = lax.all_gather(turned, 'tp', axis=0, tiled=True)]
    unnamed x52 -> x48, local copies, waits for them, and re-layouts: 3.49 us -> 7.23 us
  transfers between devices with their start and end apart: 34 -> 44, of which waited for: 12 -> 12; matrix products, arithmetic and copies ran while one was open for 8% -> 9% of each run, Pallas kernels for 0% -> 5%
where the time goes in v2:
time: 240 us; the launch traced here: 238 us
  starting transfers between devices  83.6 us (35%)
  waiting for transfers between devices  65.9 us (27%)
  blocking collectives  41.9 us (17%)
  local copies, waits for them, and re-layouts  14.5 us (6%)
  Pallas kernels  12.5 us (5%)
  matrix products  9.71 us (4%)
  other arithmetic  9.12 us (4%)
    ppermute x8, waiting for transfers between devices, body_square(): lax.ppermute(xparts[k], axes, to_piece[k])  33.8 us
    all_gather x5, blocking collectives, gather_cols(): got = lax.all_gather(value, 'tp', axis=0, axis_index_groups=sets)  29.5 us
    ppermute x8, starting transfers between devices, body_square(): gins = [lax.ppermute(gins[k], axes, by_side[k]) for k in range(n)]  22 us
    ppermute x8, starting transfers between devices, body_square(): lax.ppermute(xparts[k], axes, to_piece[k])  19.3 us
    ppermute x4, waiting for transfers between devices, scatter(): lax.ppermute(make((s - k) % n), axes, to_piece[k])  14.6 us
    ppermute x8, starting transfers between devices, maps_of(): got = [lax.ppermute(cuts[k], axes, to_piece[k]) for k in range(n)]  14.3 us
    all_gather x1, blocking collectives, body_square(): full = lax.all_gather(turned, 'tp', axis=0, tiled=True)  12.4 us
    ppermute x4, starting transfers between devices, scatter(): lax.ppermute(make((s - k) % n), axes, to_piece[k])  10.2 us
  transfers between devices with their start and end apart: 44, of which 12 were waited for; matrix products, arithmetic and copies ran while one was open for 9% of the time, Pallas kernels for 5%

profile of v2, /device:TPU:0, one launch (start us, length us, event | category | flops | bytes accessed | tf_op | source)
XLA Modules:
  0.0 238.1 jit_solution(12466434442517136321)
XLA Ops:
  0.0 1.7 collective-permute-start
  1.7 1.1 fusion.122
  2.9 1.1 copy-done.3
  6.1 0.8 fusion.127
  7.0 1.1 slice.129
  8.9 12.4 %all_gather.33 = bf16[512,512]{1,0:T(8,128)(2,1)S(1)} all-gather(bf16[128,512]{1,0:T(8,128)(2,1)S(1)} %collective-permute-done), channel_id=1, replica_groups=mesh['grp'=2,'sp'=4,'tp'=4] {'tp'}, dimensions={0}, use_global_device_ids=true | all-gather | bytes 655360 | tf_op jit(solution)/shard_map/all_gather | solution.py:182
  21.8 2.3 collective-permute-start.7
  24.1 1.4 collective-permute-start.8
  25.5 1.3 collective-permute-start.14
  26.8 2.6 %collective-permute-start.15 = (bf16[256,128]{1,0:T(8,128)(2,1)S(1)}, bf16[256,128]{1,0:T(8,128)(2,1)}, u32[]{:S(2)}, u32[]{:S(2)}) collective-permute-start(bf16[256,128]{1,0:T(8,128)(2,1)S(1)} %copy-done.14), channel_id=1, source_target_pairs={{0,3},{1,7},{2,11},{3,15},{4,0},{5,4},{6,8},{7,12},{8,1},{9,5},{10... | collective-permute-start | bytes 196616 | tf_op jit(solution)/shard_map/ppermute | solution.py:172
  29.3 0.9 convolution_convert_fusion.16
  30.3 1.0 convolution_convert_fusion.17
  31.2 0.9 convolution_convert_fusion.18
  32.2 0.9 convolution_convert_fusion.19
  34.4 0.8 copy-done.13
  35.2 1.6 collective-permute-start.16
  36.9 2.1 collective-permute-start.17
  39.7 0.9 copy.10.refs_4_
  40.5 1.6 collective-permute-start.2
  43.4 9.9 %collective-permute-start.3 = (bf16[512,128]{1,0:T(8,128)(2,1)}, bf16[512,128]{1,0:T(8,128)(2,1)S(1)}, u32[]{:S(2)}, u32[]{:S(2)}) collective-permute-start(bf16[512,128]{1,0:T(8,128)(2,1)} %convolution_convert_fusion.18), channel_id=1, source_target_pairs={{0,3},{1,7},{2,11},{3,15},{4,0},{5,4},{6,8},{7,12},{8,1},{9,5},{10... | collective-permute-start | bytes 393224 | tf_op jit(solution)/shard_map/ppermute | solution.py:202
  53.9 0.9 pad_maximum_fusion.7
  55.5 5.4 %collective-permute-done.3.refs_1_ = bf16[512,128]{1,0:T(8,128)(2,1)S(1)} collective-permute-done((bf16[512,128]{1,0:T(8,128)(2,1)}, bf16[512,128]{1,0:T(8,128)(2,1)S(1)}, u32[]{:S(2)}, u32[]{:S(2)}) %collective-permute-start.3) | collective-permute-done | bytes 131104 | tf_op jit(solution)/shard_map/ppermute | solution.py:202
  60.9 11.2 %collective-permute-done.4.refs_2_ = bf16[512,128]{1,0:T(8,128)(2,1)S(1)} collective-permute-done((bf16[512,128]{1,0:T(8,128)(2,1)}, bf16[512,128]{1,0:T(8,128)(2,1)S(1)}, u32[]{:S(2)}, u32[]{:S(2)}) %collective-permute-start.4) | collective-permute-done | bytes 131104 | tf_op jit(solution)/shard_map/ppermute | solution.py:202
  72.8 2.1 conv.2.conv_ref
  75.0 0.8 copy-done.1
  75.9 2.0 all-gather
  78.5 5.8 %collective-permute-start.11 = (bf16[512,128]{1,0:T(8,128)(2,1)S(1)}, bf16[512,128]{1,0:T(8,128)(2,1)S(1)}, u32[]{:S(2)}, u32[]{:S(2)}) collective-permute-start(bf16[512,128]{1,0:T(8,128)(2,1)S(1)} %get-tuple-element.44), channel_id=1, source_target_pairs={{0,8},{1,12},{2,2},{3,6},{4,0},{5,4},{6,10},{7,14},{8,9},{9,13},{1... | collective-permute-start | bytes 393224 | tf_op jit(solution)/shard_map/ppermute | solution.py:208
  84.3 1.9 collective-permute-start.12
  86.3 2.0 collective-permute-start.13
  89.1 4.2 %scan.2 = f32[512,128]{1,0:T(8,128)} custom-call(bf16[512,256]{1,0:T(8,128)(2,1)} %pad_maximum_fusion.6.head_ref, bf16[512,128]{1,0:T(8,128)(2,1)} %conv.2.conv_ref, bf16[256,512]{1,0:T(8,128)(2,1)} %copy_bitcast_fusion.1.maps_ref, f32[2,128]{1,0:T(2,128)} %get-tuple-element.122.coef_ref), custom_call_target="tpu_custom_call" | custom-call | tf_op jit(solution)/shard_map/scan/pallas_call | solution.py:103
  93.5 1.5 collective-permute-done.13
  94.9 1.1 fusion.32
  96.1 9.1 %all-gather.1 = bf16[2048,128]{1,0:T(8,128)(2,1)S(1)} all-gather(bf16[512,128]{1,0:T(8,128)(2,1)S(1)} %fusion.32), channel_id=3, replica_groups=mesh['grp'=2,'sp'=4,'tp'=4] {'tp'}, dimensions={0}, use_global_device_ids=true | all-gather | bytes 655360 | tf_op jit(solution)/shard_map/all_gather | solution.py:155
  107.3 4.1 %collective-permute-start.35 = (bf16[256,128]{1,0:T(8,128)(2,1)S(1)}, bf16[256,128]{1,0:T(8,128)(2,1)S(1)}, u32[]{:S(2)}, u32[]{:S(2)}) collective-permute-start(bf16[256,128]{1,0:T(8,128)(2,1)S(1)} %copy-done.18), channel_id=1, source_target_pairs={{0,3},{1,7},{2,11},{3,15},{4,0},{5,4},{6,8},{7,12},{8,1},{9,5},{10... | collective-permute-start | bytes 196616 | tf_op jit(solution)/shard_map/ppermute | solution.py:172
  111.4 2.0 collective-permute-start.37
  114.4 4.4 %collective-permute-start.19 = (bf16[512,128]{1,0:T(8,128)(2,1)S(1)}, bf16[512,128]{1,0:T(8,128)(2,1)S(1)}, u32[]{:S(2)}, u32[]{:S(2)}) collective-permute-start(bf16[512,128]{1,0:T(8,128)(2,1)S(1)} %convolution_convert_fusion.10), channel_id=1, source_target_pairs={{0,3},{1,7},{2,11},{3,15},{4,0},{5,4},{6,8},{7,12},{8,1},{9,5},{10... | collective-permute-start | bytes 393224 | tf_op jit(solution)/shard_map/ppermute | solution.py:135
  118.8 5.1 %collective-permute-start.20 = (bf16[512,128]{1,0:T(8,128)(2,1)S(1)}, bf16[512,128]{1,0:T(8,128)(2,1)S(1)}, u32[]{:S(2)}, u32[]{:S(2)}) collective-permute-start(bf16[512,128]{1,0:T(8,128)(2,1)S(1)} %convolution_convert_fusion.9), channel_id=1, source_target_pairs={{0,2},{1,6},{2,10},{3,14},{4,3},{5,7},{6,11},{7,15},{8,0},{9,4},{1... | collective-permute-start | bytes 393224 | tf_op jit(solution)/shard_map/ppermute | solution.py:135
  123.9 4.1 %collective-permute-done.36 = bf16[256,128]{1,0:T(8,128)(2,1)S(1)} collective-permute-done((bf16[256,128]{1,0:T(8,128)(2,1)S(1)}, bf16[256,128]{1,0:T(8,128)(2,1)S(1)}, u32[]{:S(2)}, u32[]{:S(2)}) %collective-permute-start.36) | collective-permute-done | bytes 65568 | tf_op jit(solution)/shard_map/ppermute | solution.py:172
  128.9 14.6 %collective-permute-done.20 = bf16[512,128]{1,0:T(8,128)(2,1)S(1)} collective-permute-done((bf16[512,128]{1,0:T(8,128)(2,1)S(1)}, bf16[512,128]{1,0:T(8,128)(2,1)S(1)}, u32[]{:S(2)}, u32[]{:S(2)}) %collective-permute-start.20) | collective-permute-done | bytes 131104 | tf_op jit(solution)/shard_map/ppermute | solution.py:135
  143.6 8.2 %all-gather.2 = bf16[2048,128]{1,0:T(8,128)(2,1)S(1)} all-gather(bf16[512,128]{1,0:T(8,128)(2,1)S(1)} %add_convert_fusion.1), channel_id=4, replica_groups=mesh['grp'=2,'sp'=4,'tp'=4] {'tp'}, dimensions={0}, use_global_device_ids=true | all-gather | bytes 655360 | tf_op jit(solution)/shard_map/all_gather | solution.py:155
  152.1 3.2 %collective-permute-start.28 = (f32[512]{0:T(512)S(1)}, f32[512]{0:T(512)S(1)}, u32[]{:S(2)}, u32[]{:S(2)}) collective-permute-start(f32[512]{0:T(512)S(1)} %get-tuple-element.67), channel_id=1, source_target_pairs={{0,8},{4,12},{8,0},{12,4},{1,9},{5,13},{9,1},{13,5},{2,10},{6,14},... | collective-permute-start | bytes 6152 | tf_op jit(solution)/shard_map/ppermute | solution.py:190
  155.3 1.1 collective-permute-start.29
  158.7 0.9 collective-permute-start.22
  160.6 3.1 %collective-permute-start.24 = (bf16[512,128]{1,0:T(8,128)(2,1)S(1)}, bf16[512,128]{1,0:T(8,128)(2,1)S(1)}, u32[]{:S(2)}, u32[]{:S(2)}) collective-permute-start(bf16[512,128]{1,0:T(8,128)(2,1)S(1)} %convolution_convert_fusion.6), channel_id=1, source_target_pairs={{0,3},{1,7},{2,11},{3,15},{4,0},{5,4},{6,8},{7,12},{8,1},{9,5},{10... | collective-permute-start | bytes 393224 | tf_op jit(solution)/shard_map/ppermute | solution.py:202
  164.3 2.9 %collective-permute-start.26 = (bf16[512,128]{1,0:T(8,128)(2,1)S(1)}, bf16[512,128]{1,0:T(8,128)(2,1)S(1)}, u32[]{:S(2)}, u32[]{:S(2)}) collective-permute-start(bf16[512,128]{1,0:T(8,128)(2,1)S(1)} %convolution_convert_fusion.4), channel_id=1, source_target_pairs={{0,1},{1,5},{2,9},{3,13},{4,2},{5,6},{6,10},{7,14},{8,3},{9,7},{10... | collective-permute-start | bytes 393224 | tf_op jit(solution)/shard_map/ppermute | solution.py:202
  167.3 0.9 copy.12.refs_4_
  168.1 17.2 %collective-permute-done.25.refs_2_ = bf16[512,128]{1,0:T(8,128)(2,1)S(1)} collective-permute-done((bf16[512,128]{1,0:T(8,128)(2,1)S(1)}, bf16[512,128]{1,0:T(8,128)(2,1)S(1)}, u32[]{:S(2)}, u32[]{:S(2)}) %collective-permute-start.25) | collective-permute-done | bytes 131104 | tf_op jit(solution)/shard_map/ppermute | solution.py:202
  186.1 2.1 conv.3.conv_ref
  188.3 0.8 copy-done
  189.2 2.0 all-gather.3
  191.8 5.8 %collective-permute-start.31 = (bf16[512,128]{1,0:T(8,128)(2,1)S(1)}, bf16[512,128]{1,0:T(8,128)(2,1)S(1)}, u32[]{:S(2)}, u32[]{:S(2)}) collective-permute-start(bf16[512,128]{1,0:T(8,128)(2,1)S(1)} %get-tuple-element.59), channel_id=1, source_target_pairs={{0,8},{1,12},{2,2},{3,6},{4,0},{5,4},{6,10},{7,14},{8,9},{9,13},{1... | collective-permute-start | bytes 393224 | tf_op jit(solution)/shard_map/ppermute | solution.py:208
  197.7 2.8 %collective-permute-start.32 = (bf16[512,128]{1,0:T(8,128)(2,1)S(1)}, bf16[512,128]{1,0:T(8,128)(2,1)S(1)}, u32[]{:S(2)}, u32[]{:S(2)}) collective-permute-start(bf16[512,128]{1,0:T(8,128)(2,1)S(1)} %get-tuple-element.60), channel_id=1, source_target_pairs={{0,1},{1,5},{2,11},{3,15},{4,9},{5,13},{6,3},{7,7},{8,0},{9,4},{10... | collective-permute-start | bytes 393224 | tf_op jit(solution)/shard_map/ppermute | solution.py:208
  200.4 2.3 collective-permute-start.33
  203.5 4.2 %scan.3 = f32[512,128]{1,0:T(8,128)} custom-call(bf16[512,256]{1,0:T(8,128)(2,1)} %pad_maximum_fusion.9.head_ref, bf16[512,128]{1,0:T(8,128)(2,1)} %conv.3.conv_ref, bf16[256,512]{1,0:T(8,128)(2,1)} %copy_bitcast_fusion.maps_ref, f32[2,128]{1,0:T(2,128)} %get-tuple-element.121.coef_ref), custom_call_target="tpu_custom_call" | custom-call | tf_op jit(solution)/shard_map/scan/pallas_call | solution.py:103
  207.7 1.4 collective-permute-done.33
  209.1 1.1 fusion.39
  210.2 8.2 %all-gather.4 = bf16[2048,128]{1,0:T(8,128)(2,1)S(1)} all-gather(bf16[512,128]{1,0:T(8,128)(2,1)S(1)} %fusion.39), channel_id=6, replica_groups=mesh['grp'=2,'sp'=4,'tp'=4] {'tp'}, dimensions={0}, use_global_device_ids=true | all-gather | bytes 655360 | tf_op jit(solution)/shard_map/all_gather | solution.py:155
  218.5 1.1 copy-done.4
  220.7 1.0 collective-permute-start.39
  221.9 2.5 %collective-permute-start.40 = (bf16[128,512]{1,0:T(8,128)(2,1)S(1)}, bf16[128,512]{1,0:T(8,128)(2,1)S(1)}, u32[]{:S(2)}, u32[]{:S(2)}) collective-permute-start(bf16[128,512]{1,0:T(8,128)(2,1)S(1)} %fusion.2), channel_id=1, source_target_pairs={{0,12},{4,0},{8,4},{12,8},{1,13},{5,1},{9,5},{13,9},{2,14},{6,2},{... | collective-permute-start | bytes 393224 | tf_op jit(solution)/shard_map/ppermute | solution.py:240
  224.4 3.8 %collective-permute-done.38 = bf16[128,512]{1,0:T(8,128)(2,1)S(1)} collective-permute-done((bf16[128,512]{1,0:T(8,128)(2,1)S(1)}, bf16[128,512]{1,0:T(8,128)(2,1)S(1)}, u32[]{:S(2)}, u32[]{:S(2)}) %collective-permute-start.38) | collective-permute-done | bytes 131104 | tf_op jit(solution)/shard_map/ppermute | solution.py:240
  228.2 5.0 %collective-permute-done.39 = bf16[128,512]{1,0:T(8,128)(2,1)S(1)} collective-permute-done((bf16[128,512]{1,0:T(8,128)(2,1)S(1)}, bf16[128,512]{1,0:T(8,128)(2,1)S(1)}, u32[]{:S(2)}, u32[]{:S(2)}) %collective-permute-start.39) | collective-permute-done | bytes 131104 | tf_op jit(solution)/shard_map/ppermute | solution.py:240
  233.7 0.9 collective-permute-start.42
  234.5 1.4 collective-permute-start.43
  (150 shorter events, 24.6 us)
Async XLA Ops:
  0.0 2.8 %copy-start.2 = (bf16[2,512,512]{2,1,0:T(8,128)(2,1)S(1)}, bf16[2,512,512]{2,1,0:T(8,128)(2,1)}, u32[]{:S(2)}) copy-start(bf16[2,512,512]{2,1,0:T(8,128)(2,1)} %param.11) | copy-start | bytes 3145732
  0.0 8.9 %collective-permute-start = (bf16[128,512]{1,0:T(8,128)(2,1)}, bf16[128,512]{1,0:T(8,128)(2,1)S(1)}, u32[]{:S(2)}, u32[]{:S(2)}) collective-permute-start(bf16[128,512]{1,0:T(8,128)(2,1)} %param.9), channel_id=1, source_target_pairs={{0,0},{1,4},{2,8},{3,12},{4,1},{5,5},{6,9},{7,13},{8,2},{9,6},{10,... | collective-permute-start | bytes 393224 | tf_op jit(solution)/shard_map/ppermute | solution.py:161
  2.8 1.2 copy-start.3
  4.0 0.7 copy-start.21
  21.4 4.1 %copy-start.15 = (bf16[256,128]{1,0:T(8,128)(2,1)S(1)}, bf16[256,128]{1,0:T(8,128)(2,1)}, u32[]{:S(2)}) copy-start(bf16[256,128]{1,0:T(8,128)(2,1)} %get-tuple-element.48) | copy-start | bytes 196612
  21.4 5.4 %copy-start.14 = (bf16[256,128]{1,0:T(8,128)(2,1)S(1)}, bf16[256,128]{1,0:T(8,128)(2,1)}, u32[]{:S(2)}) copy-start(bf16[256,128]{1,0:T(8,128)(2,1)} %get-tuple-element.49) | copy-start | bytes 196612
  21.6 12.8 %collective-permute-start.6 = (f32[512]{0:T(512)S(1)}, f32[512]{0:T(512)S(1)}, u32[]{:S(2)}, u32[]{:S(2)}) collective-permute-start(f32[512]{0:T(512)S(1)} %get-tuple-element.89), channel_id=1, source_target_pairs={{0,4},{4,8},{8,12},{12,0},{1,5},{5,9},{9,13},{13,1},{2,6},{6,10},{... | collective-permute-start | bytes 6152 | tf_op jit(solution)/shard_map/ppermute | solution.py:190
  21.8 15.1 %collective-permute-start.7 = (f32[512]{0:T(512)S(1)}, f32[512]{0:T(512)S(1)}, u32[]{:S(2)}, u32[]{:S(2)}) collective-permute-start(f32[512]{0:T(512)S(1)} %get-tuple-element.89), channel_id=1, source_target_pairs={{0,8},{4,12},{8,0},{12,4},{1,9},{5,13},{9,1},{13,5},{2,10},{6,14},... | collective-permute-start | bytes 6152 | tf_op jit(solution)/shard_map/ppermute | solution.py:190
  24.1 14.9 %collective-permute-start.8 = (f32[512]{0:T(512)S(1)}, f32[512]{0:T(512)S(1)}, u32[]{:S(2)}, u32[]{:S(2)}) collective-permute-start(f32[512]{0:T(512)S(1)} %get-tuple-element.89), channel_id=1, source_target_pairs={{0,12},{4,0},{8,4},{12,8},{1,13},{5,1},{9,5},{13,9},{2,14},{6,2},{... | collective-permute-start | bytes 6152 | tf_op jit(solution)/shard_map/ppermute | solution.py:190
  25.5 17.9 %collective-permute-start.14 = (bf16[256,128]{1,0:T(8,128)(2,1)S(1)}, bf16[256,128]{1,0:T(8,128)(2,1)}, u32[]{:S(2)}, u32[]{:S(2)}) collective-permute-start(bf16[256,128]{1,0:T(8,128)(2,1)S(1)} %copy-done.15), channel_id=1, source_target_pairs={{0,0},{1,4},{2,8},{3,12},{4,1},{5,5},{6,9},{7,13},{8,2},{9,6},{10,... | collective-permute-start | bytes 196616 | tf_op jit(solution)/shard_map/ppermute | solution.py:172
  26.8 26.5 %collective-permute-start.15 = (bf16[256,128]{1,0:T(8,128)(2,1)S(1)}, bf16[256,128]{1,0:T(8,128)(2,1)}, u32[]{:S(2)}, u32[]{:S(2)}) collective-permute-start(bf16[256,128]{1,0:T(8,128)(2,1)S(1)} %copy-done.14), channel_id=1, source_target_pairs={{0,3},{1,7},{2,11},{3,15},{4,0},{5,4},{6,8},{7,12},{8,1},{9,5},{10... | collective-permute-start | bytes 196616 | tf_op jit(solution)/shard_map/ppermute | solution.py:172
  34.4 0.8 copy-start.13
  34.4 2.5 %copy-start.12 = (bf16[256,128]{1,0:T(8,128)(2,1)S(1)}, bf16[256,128]{1,0:T(8,128)(2,1)}, u32[]{:S(2)}) copy-start(bf16[256,128]{1,0:T(8,128)(2,1)} %get-tuple-element.51) | copy-start | bytes 196612
  34.4 4.6 %copy-start.20 = (f32[2,6,512]{2,1,0:T(8,128)S(1)}, f32[2,6,512]{2,1,0:T(8,128)}, u32[]{:S(2)}) copy-start(f32[2,6,512]{2,1,0:T(8,128)} %pad_maximum_fusion.11) | copy-start | bytes 73732
  35.2 18.0 %collective-permute-start.16 = (bf16[256,128]{1,0:T(8,128)(2,1)S(1)}, bf16[256,128]{1,0:T(8,128)(2,1)S(1)}, u32[]{:S(2)}, u32[]{:S(2)}) collective-permute-start(bf16[256,128]{1,0:T(8,128)(2,1)S(1)} %copy-done.13), channel_id=1, source_target_pairs={{0,2},{1,6},{2,10},{3,14},{4,3},{5,7},{6,11},{7,15},{8,0},{9,4},{1... | collective-permute-start | bytes 196616 | tf_op jit(solution)/shard_map/ppermute | solution.py:172
  36.9 17.0 %collective-permute-start.17 = (bf16[256,128]{1,0:T(8,128)(2,1)S(1)}, bf16[256,128]{1,0:T(8,128)(2,1)S(1)}, u32[]{:S(2)}, u32[]{:S(2)}) collective-permute-start(bf16[256,128]{1,0:T(8,128)(2,1)S(1)} %copy-done.12), channel_id=1, source_target_pairs={{0,1},{1,5},{2,9},{3,13},{4,2},{5,6},{6,10},{7,14},{8,3},{9,7},{10... | collective-permute-start | bytes 196616 | tf_op jit(solution)/shard_map/ppermute | solution.py:172
  39.0 1.5 collective-permute-start.9
  40.5 15.0 %collective-permute-start.2 = (bf16[512,128]{1,0:T(8,128)(2,1)}, bf16[512,128]{1,0:T(8,128)(2,1)S(1)}, u32[]{:S(2)}, u32[]{:S(2)}) collective-permute-start(bf16[512,128]{1,0:T(8,128)(2,1)} %convolution_convert_fusion.19), channel_id=1, source_target_pairs={{0,0},{1,4},{2,8},{3,12},{4,1},{5,5},{6,9},{7,13},{8,2},{9,6},{10,... | collective-permute-start | bytes 393224 | tf_op jit(solution)/shard_map/ppermute | solution.py:202
  43.4 17.5 %collective-permute-start.3 = (bf16[512,128]{1,0:T(8,128)(2,1)}, bf16[512,128]{1,0:T(8,128)(2,1)S(1)}, u32[]{:S(2)}, u32[]{:S(2)}) collective-permute-start(bf16[512,128]{1,0:T(8,128)(2,1)} %convolution_convert_fusion.18), channel_id=1, source_target_pairs={{0,3},{1,7},{2,11},{3,15},{4,0},{5,4},{6,8},{7,12},{8,1},{9,5},{10... | collective-permute-start | bytes 393224 | tf_op jit(solution)/shard_map/ppermute | solution.py:202
  53.3 18.9 %collective-permute-start.4 = (bf16[512,128]{1,0:T(8,128)(2,1)}, bf16[512,128]{1,0:T(8,128)(2,1)S(1)}, u32[]{:S(2)}, u32[]{:S(2)}) collective-permute-start(bf16[512,128]{1,0:T(8,128)(2,1)} %convolution_convert_fusion.17), channel_id=1, source_target_pairs={{0,2},{1,6},{2,10},{3,14},{4,3},{5,7},{6,11},{7,15},{8,0},{9,4},{1... | collective-permute-start | bytes 393224 | tf_op jit(solution)/shard_map/ppermute | solution.py:202
  53.3 18.9 %collective-permute-start.5 = (bf16[512,128]{1,0:T(8,128)(2,1)}, bf16[512,128]{1,0:T(8,128)(2,1)}, u32[]{:S(2)}, u32[]{:S(2)}) collective-permute-start(bf16[512,128]{1,0:T(8,128)(2,1)} %convolution_convert_fusion.16), channel_id=1, source_target_pairs={{0,1},{1,5},{2,9},{3,13},{4,2},{5,6},{6,10},{7,14},{8,3},{9,7},{10... | collective-permute-start | bytes 393224 | tf_op jit(solution)/shard_map/ppermute | solution.py:202
  53.9 21.0 %collective-permute-start.1 = (bf16[2,512,128]{2,1,0:T(8,128)(2,1)S(1)}, bf16[2,512,128]{2,1,0:T(8,128)(2,1)S(1)}, u32[]{:S(2)}, u32[]{:S(2)}) collective-permute-start(bf16[2,512,128]{2,1,0:T(8,128)(2,1)S(1)} %pad_maximum_fusion.5), channel_id=1, source_target_pairs={{0,2},{1,3},{2,0},{3,1},{4,6},{5,7},{6,4},{7,5},{8,10},{9,11},{10,... | collective-permute-start | bytes 786440 | tf_op jit(solution)/shard_map/ppermute | solution.py:150
  55.5 16.6 %copy-start.5 = (bf16[512,128]{1,0:T(8,128)(2,1)}, bf16[512,128]{1,0:T(8,128)(2,1)S(1)}, u32[]{:S(2)}) copy-start(bf16[512,128]{1,0:T(8,128)(2,1)S(1)} %collective-permute-done.2.refs_0_) | copy-start | bytes 393220
  60.9 11.2 %copy-start.6 = (bf16[512,128]{1,0:T(8,128)(2,1)}, bf16[512,128]{1,0:T(8,128)(2,1)S(1)}, u32[]{:S(2)}) copy-start(bf16[512,128]{1,0:T(8,128)(2,1)S(1)} %collective-permute-done.3.refs_1_) | copy-start | bytes 393220
  75.0 0.9 copy-start.1
  77.9 15.4 %collective-permute-start.10 = (bf16[512,128]{1,0:T(8,128)(2,1)S(1)}, bf16[512,128]{1,0:T(8,128)(2,1)S(1)}, u32[]{:S(2)}, u32[]{:S(2)}) collective-permute-start(bf16[512,128]{1,0:T(8,128)(2,1)S(1)} %get-tuple-element.43), channel_id=1, source_target_pairs={{0,0},{1,4},{2,10},{3,14},{4,8},{5,12},{6,2},{7,6},{8,1},{9,5},{10... | collective-permute-start | bytes 393224 | tf_op jit(solution)/shard_map/ppermute | solution.py:208
  78.5 14.7 %collective-permute-start.11 = (bf16[512,128]{1,0:T(8,128)(2,1)S(1)}, bf16[512,128]{1,0:T(8,128)(2,1)S(1)}, u32[]{:S(2)}, u32[]{:S(2)}) collective-permute-start(bf16[512,128]{1,0:T(8,128)(2,1)S(1)} %get-tuple-element.44), channel_id=1, source_target_pairs={{0,8},{1,12},{2,2},{3,6},{4,0},{5,4},{6,10},{7,14},{8,9},{9,13},{1... | collective-permute-start | bytes 393224 | tf_op jit(solution)/shard_map/ppermute | solution.py:208
  84.3 9.1 %collective-permute-start.12 = (bf16[512,128]{1,0:T(8,128)(2,1)S(1)}, bf16[512,128]{1,0:T(8,128)(2,1)S(1)}, u32[]{:S(2)}, u32[]{:S(2)}) collective-permute-start(bf16[512,128]{1,0:T(8,128)(2,1)S(1)} %get-tuple-element.45), channel_id=1, source_target_pairs={{0,1},{1,5},{2,11},{3,15},{4,9},{5,13},{6,3},{7,7},{8,0},{9,4},{10... | collective-permute-start | bytes 393224 | tf_op jit(solution)/shard_map/ppermute | solution.py:208
  86.3 8.7 %collective-permute-start.13 = (bf16[512,128]{1,0:T(8,128)(2,1)S(1)}, bf16[512,128]{1,0:T(8,128)(2,1)S(1)}, u32[]{:S(2)}, u32[]{:S(2)}) collective-permute-start(bf16[512,128]{1,0:T(8,128)(2,1)S(1)} %get-tuple-element.46), channel_id=1, source_target_pairs={{0,9},{1,13},{2,3},{3,7},{4,1},{5,5},{6,11},{7,15},{8,8},{9,12},{1... | collective-permute-start | bytes 393224 | tf_op jit(solution)/shard_map/ppermute | solution.py:208
  105.8 0.8 copy-start.19
  105.8 1.5 copy-start.18
  105.8 5.6 %copy-start.17 = (bf16[256,128]{1,0:T(8,128)(2,1)S(1)}, bf16[256,128]{1,0:T(8,128)(2,1)}, u32[]{:S(2)}) copy-start(bf16[256,128]{1,0:T(8,128)(2,1)} %get-tuple-element.65) | copy-start | bytes 196612
  105.8 5.6 %copy-start.16 = (bf16[256,128]{1,0:T(8,128)(2,1)S(1)}, bf16[256,128]{1,0:T(8,128)(2,1)}, u32[]{:S(2)}) copy-start(bf16[256,128]{1,0:T(8,128)(2,1)} %get-tuple-element.66) | copy-start | bytes 196612
  106.6 7.7 %collective-permute-start.34 = (bf16[256,128]{1,0:T(8,128)(2,1)S(1)}, bf16[256,128]{1,0:T(8,128)(2,1)S(1)}, u32[]{:S(2)}, u32[]{:S(2)}) collective-permute-start(bf16[256,128]{1,0:T(8,128)(2,1)S(1)} %copy-done.19), channel_id=1, source_target_pairs={{0,0},{1,4},{2,8},{3,12},{4,1},{5,5},{6,9},{7,13},{8,2},{9,6},{10,... | collective-permute-start | bytes 196616 | tf_op jit(solution)/shard_map/ppermute | solution.py:172
  107.3 11.5 %collective-permute-start.35 = (bf16[256,128]{1,0:T(8,128)(2,1)S(1)}, bf16[256,128]{1,0:T(8,128)(2,1)S(1)}, u32[]{:S(2)}, u32[]{:S(2)}) collective-permute-start(bf16[256,128]{1,0:T(8,128)(2,1)S(1)} %copy-done.18), channel_id=1, source_target_pairs={{0,3},{1,7},{2,11},{3,15},{4,0},{5,4},{6,8},{7,12},{8,1},{9,5},{10... | collective-permute-start | bytes 196616 | tf_op jit(solution)/shard_map/ppermute | solution.py:172
  111.4 16.6 %collective-permute-start.36 = (bf16[256,128]{1,0:T(8,128)(2,1)S(1)}, bf16[256,128]{1,0:T(8,128)(2,1)S(1)}, u32[]{:S(2)}, u32[]{:S(2)}) collective-permute-start(bf16[256,128]{1,0:T(8,128)(2,1)S(1)} %copy-done.17), channel_id=1, source_target_pairs={{0,2},{1,6},{2,10},{3,14},{4,3},{5,7},{6,11},{7,15},{8,0},{9,4},{1... | collective-permute-start | bytes 196616 | tf_op jit(solution)/shard_map/ppermute | solution.py:172
  111.4 16.6 %collective-permute-start.37 = (bf16[256,128]{1,0:T(8,128)(2,1)S(1)}, bf16[256,128]{1,0:T(8,128)(2,1)S(1)}, u32[]{:S(2)}, u32[]{:S(2)}) collective-permute-start(bf16[256,128]{1,0:T(8,128)(2,1)S(1)} %copy-done.16), channel_id=1, source_target_pairs={{0,1},{1,5},{2,9},{3,13},{4,2},{5,6},{6,10},{7,14},{8,3},{9,7},{10... | collective-permute-start | bytes 196616 | tf_op jit(solution)/shard_map/ppermute | solution.py:172
  113.4 15.5 %collective-permute-start.18 = (bf16[512,128]{1,0:T(8,128)(2,1)S(1)}, bf16[512,128]{1,0:T(8,128)(2,1)S(1)}, u32[]{:S(2)}, u32[]{:S(2)}) collective-permute-start(bf16[512,128]{1,0:T(8,128)(2,1)S(1)} %convolution_convert_fusion.11), channel_id=1, source_target_pairs={{0,0},{1,4},{2,8},{3,12},{4,1},{5,5},{6,9},{7,13},{8,2},{9,6},{10,... | collective-permute-start | bytes 393224 | tf_op jit(solution)/shard_map/ppermute | solution.py:135
  114.4 14.5 %collective-permute-start.19 = (bf16[512,128]{1,0:T(8,128)(2,1)S(1)}, bf16[512,128]{1,0:T(8,128)(2,1)S(1)}, u32[]{:S(2)}, u32[]{:S(2)}) collective-permute-start(bf16[512,128]{1,0:T(8,128)(2,1)S(1)} %convolution_convert_fusion.10), channel_id=1, source_target_pairs={{0,3},{1,7},{2,11},{3,15},{4,0},{5,4},{6,8},{7,12},{8,1},{9,5},{10... | collective-permute-start | bytes 393224 | tf_op jit(solution)/shard_map/ppermute | solution.py:135
  118.8 24.7 %collective-permute-start.20 = (bf16[512,128]{1,0:T(8,128)(2,1)S(1)}, bf16[512,128]{1,0:T(8,128)(2,1)S(1)}, u32[]{:S(2)}, u32[]{:S(2)}) collective-permute-start(bf16[512,128]{1,0:T(8,128)(2,1)S(1)} %convolution_convert_fusion.9), channel_id=1, source_target_pairs={{0,2},{1,6},{2,10},{3,14},{4,3},{5,7},{6,11},{7,15},{8,0},{9,4},{1... | collective-permute-start | bytes 393224 | tf_op jit(solution)/shard_map/ppermute | solution.py:135
  128.0 15.5 %collective-permute-start.21 = (bf16[512,128]{1,0:T(8,128)(2,1)S(1)}, bf16[512,128]{1,0:T(8,128)(2,1)S(1)}, u32[]{:S(2)}, u32[]{:S(2)}) collective-permute-start(bf16[512,128]{1,0:T(8,128)(2,1)S(1)} %convolution_convert_fusion.8), channel_id=1, source_target_pairs={{0,1},{1,5},{2,9},{3,13},{4,2},{5,6},{6,10},{7,14},{8,3},{9,7},{10... | collective-permute-start | bytes 393224 | tf_op jit(solution)/shard_map/ppermute | solution.py:135
  152.0 8.6 %collective-permute-start.27 = (f32[512]{0:T(512)S(1)}, f32[512]{0:T(512)S(1)}, u32[]{:S(2)}, u32[]{:S(2)}) collective-permute-start(f32[512]{0:T(512)S(1)} %get-tuple-element.67), channel_id=1, source_target_pairs={{0,4},{4,8},{8,12},{12,0},{1,5},{5,9},{9,13},{13,1},{2,6},{6,10},{... | collective-permute-start | bytes 6152 | tf_op jit(solution)/shard_map/ppermute | solution.py:190
  152.1 11.6 %collective-permute-start.28 = (f32[512]{0:T(512)S(1)}, f32[512]{0:T(512)S(1)}, u32[]{:S(2)}, u32[]{:S(2)}) collective-permute-start(f32[512]{0:T(512)S(1)} %get-tuple-element.67), channel_id=1, source_target_pairs={{0,8},{4,12},{8,0},{12,4},{1,9},{5,13},{9,1},{13,5},{2,10},{6,14},... | collective-permute-start | bytes 6152 | tf_op jit(solution)/shard_map/ppermute | solution.py:190
  155.3 9.0 %collective-permute-start.29 = (f32[512]{0:T(512)S(1)}, f32[512]{0:T(512)S(1)}, u32[]{:S(2)}, u32[]{:S(2)}) collective-permute-start(f32[512]{0:T(512)S(1)} %get-tuple-element.67), channel_id=1, source_target_pairs={{0,12},{4,0},{8,4},{12,8},{1,13},{5,1},{9,5},{13,9},{2,14},{6,2},{... | collective-permute-start | bytes 6152 | tf_op jit(solution)/shard_map/ppermute | solution.py:190
  158.7 29.4 %collective-permute-start.22 = (bf16[2,512,128]{2,1,0:T(8,128)(2,1)S(1)}, bf16[2,512,128]{2,1,0:T(8,128)(2,1)S(1)}, u32[]{:S(2)}, u32[]{:S(2)}) collective-permute-start(bf16[2,512,128]{2,1,0:T(8,128)(2,1)S(1)} %pad_maximum_fusion.8), channel_id=1, source_target_pairs={{0,2},{1,3},{2,0},{3,1},{4,6},{5,7},{6,4},{7,5},{8,10},{9,11},{10,... | collective-permute-start | bytes 786440 | tf_op jit(solution)/shard_map/ppermute | solution.py:150
  159.9 8.2 %collective-permute-start.23 = (bf16[512,128]{1,0:T(8,128)(2,1)S(1)}, bf16[512,128]{1,0:T(8,128)(2,1)S(1)}, u32[]{:S(2)}, u32[]{:S(2)}) collective-permute-start(bf16[512,128]{1,0:T(8,128)(2,1)S(1)} %convolution_convert_fusion.7), channel_id=1, source_target_pairs={{0,0},{1,4},{2,8},{3,12},{4,1},{5,5},{6,9},{7,13},{8,2},{9,6},{10,... | collective-permute-start | bytes 393224 | tf_op jit(solution)/shard_map/ppermute | solution.py:202
  160.6 7.5 %collective-permute-start.24 = (bf16[512,128]{1,0:T(8,128)(2,1)S(1)}, bf16[512,128]{1,0:T(8,128)(2,1)S(1)}, u32[]{:S(2)}, u32[]{:S(2)}) collective-permute-start(bf16[512,128]{1,0:T(8,128)(2,1)S(1)} %convolution_convert_fusion.6), channel_id=1, source_target_pairs={{0,3},{1,7},{2,11},{3,15},{4,0},{5,4},{6,8},{7,12},{8,1},{9,5},{10... | collective-permute-start | bytes 393224 | tf_op jit(solution)/shard_map/ppermute | solution.py:202
  163.7 21.6 %collective-permute-start.25 = (bf16[512,128]{1,0:T(8,128)(2,1)S(1)}, bf16[512,128]{1,0:T(8,128)(2,1)S(1)}, u32[]{:S(2)}, u32[]{:S(2)}) collective-permute-start(bf16[512,128]{1,0:T(8,128)(2,1)S(1)} %convolution_convert_fusion.5), channel_id=1, source_target_pairs={{0,2},{1,6},{2,10},{3,14},{4,3},{5,7},{6,11},{7,15},{8,0},{9,4},{1... | collective-permute-start | bytes 393224 | tf_op jit(solution)/shard_map/ppermute | solution.py:202
  164.3 21.0 %collective-permute-start.26 = (bf16[512,128]{1,0:T(8,128)(2,1)S(1)}, bf16[512,128]{1,0:T(8,128)(2,1)S(1)}, u32[]{:S(2)}, u32[]{:S(2)}) collective-permute-start(bf16[512,128]{1,0:T(8,128)(2,1)S(1)} %convolution_convert_fusion.4), channel_id=1, source_target_pairs={{0,1},{1,5},{2,9},{3,13},{4,2},{5,6},{6,10},{7,14},{8,3},{9,7},{10... | collective-permute-start | bytes 393224 | tf_op jit(solution)/shard_map/ppermute | solution.py:202
  168.1 17.2 %copy-start.8 = (bf16[512,128]{1,0:T(8,128)(2,1)}, bf16[512,128]{1,0:T(8,128)(2,1)S(1)}, u32[]{:S(2)}) copy-start(bf16[512,128]{1,0:T(8,128)(2,1)S(1)} %collective-permute-done.23.refs_0_) | copy-start | bytes 393220
  168.1 17.2 %copy-start.9 = (bf16[512,128]{1,0:T(8,128)(2,1)}, bf16[512,128]{1,0:T(8,128)(2,1)S(1)}, u32[]{:S(2)}) copy-start(bf16[512,128]{1,0:T(8,128)(2,1)S(1)} %collective-permute-done.24.refs_1_) | copy-start | bytes 393220
  188.3 0.9 copy-start
  191.2 16.5 %collective-permute-start.30 = (bf16[512,128]{1,0:T(8,128)(2,1)S(1)}, bf16[512,128]{1,0:T(8,128)(2,1)S(1)}, u32[]{:S(2)}, u32[]{:S(2)}) collective-permute-start(bf16[512,128]{1,0:T(8,128)(2,1)S(1)} %get-tuple-element.58), channel_id=1, source_target_pairs={{0,0},{1,4},{2,10},{3,14},{4,8},{5,12},{6,2},{7,6},{8,1},{9,5},{10... | collective-permute-start | bytes 393224 | tf_op jit(solution)/shard_map/ppermute | solution.py:208
  191.8 15.9 %collective-permute-start.31 = (bf16[512,128]{1,0:T(8,128)(2,1)S(1)}, bf16[512,128]{1,0:T(8,128)(2,1)S(1)}, u32[]{:S(2)}, u32[]{:S(2)}) collective-permute-start(bf16[512,128]{1,0:T(8,128)(2,1)S(1)} %get-tuple-element.59), channel_id=1, source_target_pairs={{0,8},{1,12},{2,2},{3,6},{4,0},{5,4},{6,10},{7,14},{8,9},{9,13},{1... | collective-permute-start | bytes 393224 | tf_op jit(solution)/shard_map/ppermute | solution.py:208
  197.7 10.0 %collective-permute-start.32 = (bf16[512,128]{1,0:T(8,128)(2,1)S(1)}, bf16[512,128]{1,0:T(8,128)(2,1)S(1)}, u32[]{:S(2)}, u32[]{:S(2)}) collective-permute-start(bf16[512,128]{1,0:T(8,128)(2,1)S(1)} %get-tuple-element.60), channel_id=1, source_target_pairs={{0,1},{1,5},{2,11},{3,15},{4,9},{5,13},{6,3},{7,7},{8,0},{9,4},{10... | collective-permute-start | bytes 393224 | tf_op jit(solution)/shard_map/ppermute | solution.py:208
  200.4 8.7 %collective-permute-start.33 = (bf16[512,128]{1,0:T(8,128)(2,1)S(1)}, bf16[512,128]{1,0:T(8,128)(2,1)S(1)}, u32[]{:S(2)}, u32[]{:S(2)}) collective-permute-start(bf16[512,128]{1,0:T(8,128)(2,1)S(1)} %get-tuple-element.61), channel_id=1, source_target_pairs={{0,9},{1,13},{2,3},{3,7},{4,1},{5,5},{6,11},{7,15},{8,8},{9,12},{1... | collective-permute-start | bytes 393224 | tf_op jit(solution)/shard_map/ppermute | solution.py:208
  218.4 1.2 copy-start.4
  219.9 8.3 %collective-permute-start.38 = (bf16[128,512]{1,0:T(8,128)(2,1)S(1)}, bf16[128,512]{1,0:T(8,128)(2,1)S(1)}, u32[]{:S(2)}, u32[]{:S(2)}) collective-permute-start(bf16[128,512]{1,0:T(8,128)(2,1)S(1)} %fusion), channel_id=1, source_target_pairs={{0,4},{4,8},{8,12},{12,0},{1,5},{5,9},{9,13},{13,1},{2,6},{6,10},{... | collective-permute-start | bytes 393224 | tf_op jit(solution)/shard_map/ppermute | solution.py:240
  220.7 12.6 %collective-permute-start.39 = (bf16[128,512]{1,0:T(8,128)(2,1)S(1)}, bf16[128,512]{1,0:T(8,128)(2,1)S(1)}, u32[]{:S(2)}, u32[]{:S(2)}) collective-permute-start(bf16[128,512]{1,0:T(8,128)(2,1)S(1)} %fusion.1), channel_id=1, source_target_pairs={{0,8},{4,12},{8,0},{12,4},{1,9},{5,13},{9,1},{13,5},{2,10},{6,14},... | collective-permute-start | bytes 393224 | tf_op jit(solution)/shard_map/ppermute | solution.py:240
  221.9 11.3 %collective-permute-start.40 = (bf16[128,512]{1,0:T(8,128)(2,1)S(1)}, bf16[128,512]{1,0:T(8,128)(2,1)S(1)}, u32[]{:S(2)}, u32[]{:S(2)}) collective-permute-start(bf16[128,512]{1,0:T(8,128)(2,1)S(1)} %fusion.2), channel_id=1, source_target_pairs={{0,12},{4,0},{8,4},{12,8},{1,13},{5,1},{9,5},{13,9},{2,14},{6,2},{... | collective-permute-start | bytes 393224 | tf_op jit(solution)/shard_map/ppermute | solution.py:240
  233.6 3.7 %copy-start.23 = (f32[512]{0:T(512)S(1)}, f32[512]{0:T(512)}, u32[]{:S(2)}) copy-start(f32[512]{0:T(512)} %param.17) | copy-start | bytes 6148
  233.6 3.0 %collective-permute-start.41 = (f32[128]{0:T(128)S(1)}, f32[128]{0:T(128)S(1)}, u32[]{:S(2)}, u32[]{:S(2)}) collective-permute-start(f32[128]{0:T(128)S(1)} %get-tuple-element.127), channel_id=1, source_target_pairs={{0,1},{1,2},{2,3},{3,0},{4,5},{5,6},{6,7},{7,4},{8,9},{9,10},{10,1... | collective-permute-start | bytes 1544 | tf_op jit(solution)/shard_map/ppermute | solution.py:249
  233.7 3.6 %collective-permute-start.42 = (f32[128]{0:T(128)S(1)}, f32[128]{0:T(128)S(1)}, u32[]{:S(2)}, u32[]{:S(2)}) collective-permute-start(f32[128]{0:T(128)S(1)} %get-tuple-element.127), channel_id=1, source_target_pairs={{0,2},{1,3},{2,0},{3,1},{4,6},{5,7},{6,4},{7,5},{8,10},{9,11},{10,... | collective-permute-start | bytes 1544 | tf_op jit(solution)/shard_map/ppermute | solution.py:249
  234.5 2.8 %collective-permute-start.43 = (f32[128]{0:T(128)S(1)}, f32[128]{0:T(128)S(1)}, u32[]{:S(2)}, u32[]{:S(2)}) collective-permute-start(f32[128]{0:T(128)S(1)} %get-tuple-element.127), channel_id=1, source_target_pairs={{0,3},{1,0},{2,1},{3,2},{4,7},{5,4},{6,5},{7,6},{8,11},{9,8},{10,9... | collective-permute-start | bytes 1544 | tf_op jit(solution)/shard_map/ppermute | solution.py:249
  (4 other events, 2.7 us)
